TPU v7x, 128 devices: a whole 4x4x4 slice. The times are simulated.
128 devices in a mesh: sp: 16 (over z, x), tp: 8 (over y, core).
Axes of the slice: x: 4, y: 4, z: 4, core: 2. Of those that a mesh axis runs over, the one named last changes fastest.
Arguments:
- residual: bfloat16 [8192, 2048], P(('sp', 'tp')), may hold values from -6 to 6
- query_small: bfloat16 [8192, 8, 128], P('sp', 'tp'), may hold values from -120 to 120
- key_small: bfloat16 [8192, 8, 128], P('sp', 'tp'), may hold values from -6 to 6
- value_small: bfloat16 [8192, 8, 128], P('sp', 'tp'), may hold values from -6 to 6
- query_large: bfloat16 [8192, 8, 256], P('sp', 'tp'), may hold values from -120 to 120
- key_large: bfloat16 [8192, 8, 256], P('sp', 'tp'), may hold values from -6 to 6
- value_large: bfloat16 [8192, 8, 128], P('sp', 'tp'), may hold values from -6 to 6
- lambda_small: float32 [8], P('tp'), may hold values from 0.3 to 0.8
- lambda_large: float32 [8], P('tp'), may hold values from 0.3 to 0.8
- head_gain: float32 [128], replicated, may hold values from 0.1 to 1.9
- output_small: bfloat16 [1024, 2048], P('tp'), may hold values from -0.125 to 0.125
- output_large: bfloat16 [1024, 2048], P('tp'), may hold values from -0.125 to 0.125
- norm_gain: float32 [2048], replicated, may hold values from 0.1 to 1.9
- gate_weight: bfloat16 [2048, 5632], P('sp', 'tp'), may hold values from -0.125 to 0.125
- up_weight: bfloat16 [2048, 5632], P('sp', 'tp'), may hold values from -0.125 to 0.125
- down_weight: bfloat16 [5632, 2048], P('tp', 'sp'), may hold values from -0.3125 to 0.3125
Outputs:
- block_output: bfloat16 [8192, 2048], P(('sp', 'tp'))
All inputs are finite; a program needn't handle non-finite values.
Results may differ from a plain program's by a relative error of at most 0.015.
Values may be sent and summed in bfloat16 or wider, within the bound.
A program may use at most 128 MiB of HBM per device.

v0:
```python
import math

import jax
import jax.numpy as jnp
from jax import lax
from jax.sharding import PartitionSpec as P

residual_scale = 8.0**0.25
branch_scale = 0.8
norm_epsilon = 1e-05
masked_score = -1e30


def rows_first(arrays, axis, dims):
    turned = [jnp.moveaxis(a, dim, 0) for a, dim in zip(arrays, dims)]
    both = jnp.concatenate([t.reshape(len(t), -1) for t in turned], axis=1)
    whole, at, finished = (lax.all_gather(both, axis, axis=0, tiled=True), 0, [])
    for t, dim in zip(turned, dims):
        share = whole[:, at : at + t[0].size].reshape(-1, *t.shape[1:])
        finished.append(jnp.moveaxis(share, 0, dim))
        at += t[0].size
    return tuple(finished)


def side_by_side(arrays, axis, dim, along):
    ends, at = ([], 0)
    for a in arrays[:-1]:
        at += a.shape[along]
        ends.append(at)
    both = jnp.concatenate(arrays, axis=along)
    return tuple(jnp.split(lax.all_gather(both, axis, axis=dim, tiled=True), ends, axis=along))


def split_up(array, dim, devices):
    before, after = (array.shape[:dim], array.shape[dim + 1 :])
    return jnp.moveaxis(array.reshape(*before, devices, -1, *after), dim, 0)


def sent_and_summed(array, axis, dim):
    devices = lax.axis_size(axis)
    tiles = lax.all_to_all(split_up(array, dim, devices), axis, 0, 0, tiled=True)
    return jnp.sum(tiles.astype(jnp.float32), axis=0)


def in_order(tiles, dim):
    dims = list(tiles.shape[1:])
    dims[dim] *= tiles.shape[0]
    return jnp.moveaxis(tiles, 0, dim).reshape(dims)


def from_everyone(array, axis):
    devices = lax.axis_size(axis)
    return lax.all_to_all(
        jnp.broadcast_to(array[None], (devices, *array.shape)), axis, 0, 0, tiled=True
    )


def gathered_copies(array, axis, dim):
    return in_order(from_everyone(array, axis), dim)


def layer_norm(values, gains):
    centered = values - jnp.mean(values, axis=-1, keepdims=True)
    variance = jnp.mean(centered * centered, axis=-1, keepdims=True)
    return centered * lax.rsqrt(variance + norm_epsilon) * gains


def empty_state(head_count, tokens, width):
    return (
        jnp.full((head_count, 2, tokens), masked_score, jnp.float32),
        jnp.zeros((head_count, 2, tokens), jnp.float32),
        jnp.zeros((head_count, 2, tokens, width), jnp.float32),
    )


def absorb_group(state, query_maps, key_block, value_block, key_index, query_index):
    running_max, totals, accumulated = state
    head_size = query_maps.shape[3]
    scores = jnp.einsum(
        "qhmd,khmd->hmqk", query_maps, key_block, preferred_element_type=jnp.float32
    ) * head_size ** (-0.5)
    visible = key_index[None, :] <= query_index[:, None]
    scores = jnp.where(visible, scores, masked_score)
    new_max = jnp.maximum(running_max, jnp.max(scores, axis=-1))
    fading = jnp.exp(running_max - new_max)
    weights = jnp.where(visible, jnp.exp(scores - new_max[..., None]), 0.0)
    totals = totals * fading + jnp.sum(weights, axis=-1)
    accumulated = accumulated * fading[..., None] + jnp.einsum(
        "hmqk,khe->hmqe",
        weights.astype(jnp.bfloat16),
        value_block,
        preferred_element_type=jnp.float32,
    )
    return (new_max, totals, accumulated)


def finish_group(state, lambdas, head_gain):
    running_max, totals, accumulated = state
    map_out = accumulated / totals[..., None]
    combined = map_out[:, 0] - lambdas[:, None, None] * map_out[:, 1]
    mean_square = jnp.mean(combined * combined, axis=-1, keepdims=True)
    normed = (combined * lax.rsqrt(mean_square + norm_epsilon) * head_gain * branch_scale).astype(
        jnp.bfloat16
    )
    head_count, tokens, width = normed.shape
    return jnp.transpose(normed, (1, 0, 2)).reshape(tokens, head_count * width)


def per_device(
    residual,
    query_small,
    key_small,
    value_small,
    query_large,
    key_large,
    value_large,
    lambda_small,
    lambda_large,
    head_gain,
    output_small,
    output_large,
    norm_gain,
    gate_weight,
    up_weight,
    down_weight,
):
    tokens = query_small.shape[0]
    half = tokens // 2
    gate_full, up_full, down_full = rows_first(
        (gate_weight, up_weight, down_weight), "sp", (0, 0, 1)
    )
    heads_small = query_small.shape[1]
    heads_large = query_large.shape[1]
    value_width = value_small.shape[2]
    first_start = lax.axis_index("sp") * tokens
    later_small = query_small[half:]
    later_large = query_large[half:]
    second_start = first_start + half
    halves = (
        (
            query_small[:half].reshape(half, heads_small, 2, -1),
            query_large[:half].reshape(half, heads_large, 2, -1),
            first_start + jnp.arange(half, dtype=jnp.int32),
        ),
        (
            later_small.reshape(half, heads_small, 2, -1),
            later_large.reshape(half, heads_large, 2, -1),
            second_start + jnp.arange(half, dtype=jnp.int32),
        ),
    )
    one_half = (
        empty_state(heads_small, half, value_width),
        empty_state(heads_large, half, value_width),
    )
    keys_first, keys_second, values_first, values_second = side_by_side(
        (key_small, key_large, value_small, value_large), "sp", 0, 2
    )
    row_count = keys_first.shape[0]
    block_size = math.gcd(row_count, 512)
    number = row_count // block_size
    stacked = (
        keys_first.reshape(number, block_size, heads_small, 2, -1),
        keys_second.reshape(number, block_size, heads_large, 2, -1),
        values_first.reshape(number, block_size, heads_small, value_width),
        values_second.reshape(number, block_size, heads_large, value_width),
    )

    def step(carried, block_items):
        block_index, blocks = block_items
        key_index = block_index * block_size + jnp.arange(block_size, dtype=jnp.int32)
        updated = []
        for which in range(2):
            maps_small, maps_large, query_index = halves[which]

            def take(pair):
                return (
                    absorb_group(pair[0], maps_small, blocks[0], blocks[2], key_index, query_index),
                    absorb_group(pair[1], maps_large, blocks[1], blocks[3], key_index, query_index),
                )

            def leave(pair):
                return pair

            updated.append(
                lax.cond(key_index[0] <= query_index[half - 1], take, leave, carried[which])
            )
        return ((updated[0], updated[1]), None)

    result, unused = lax.scan(
        step, (one_half, one_half), (jnp.arange(number, dtype=jnp.int32), stacked)
    )
    first_states, second_states = result
    early_small = finish_group(first_states[0], lambda_small, head_gain)
    early_large = finish_group(first_states[1], lambda_large, head_gain)
    late_small = finish_group(second_states[0], lambda_small, head_gain)
    late_large = finish_group(second_states[1], lambda_large, head_gain)
    attended_small = jnp.concatenate([early_small, late_small], axis=0)
    attended_large = jnp.concatenate([early_large, late_large], axis=0)
    mixed_sum = sent_and_summed(
        (
            jnp.dot(attended_small, output_small, preferred_element_type=jnp.float32)
            + jnp.dot(attended_large, output_large, preferred_element_type=jnp.float32)
        ).astype(jnp.bfloat16),
        "tp",
        0,
    )
    normed = layer_norm(
        residual_scale * residual.astype(jnp.float32) + mixed_sum, norm_gain
    ).astype(jnp.bfloat16)
    whole_rows = gathered_copies(normed, "tp", 0)
    gate_rows = jnp.dot(whole_rows, gate_full, preferred_element_type=jnp.float32)
    up_rows = jnp.dot(whole_rows, up_full, preferred_element_type=jnp.float32)
    hidden = (jax.nn.silu(gate_rows) * up_rows).astype(jnp.bfloat16)
    down_sum = sent_and_summed(
        jnp.dot(hidden, down_full, preferred_element_type=jnp.float32).astype(jnp.bfloat16), "tp", 0
    )
    return (residual_scale * normed.astype(jnp.float32) + 0.5 * down_sum).astype(jnp.bfloat16)


def solution(mesh):
    in_specs = (
        P(("sp", "tp"), None),
        P("sp", "tp", None),
        P("sp", "tp", None),
        P("sp", "tp", None),
        P("sp", "tp", None),
        P("sp", "tp", None),
        P("sp", "tp", None),
        P("tp"),
        P("tp"),
        P(),
        P("tp", None),
        P("tp", None),
        P(),
        P("sp", "tp"),
        P("sp", "tp"),
        P("tp", "sp"),
    )
    out_specs = P(("sp", "tp"), None)
    return jax.shard_map(
        per_device, mesh=mesh, in_specs=in_specs, out_specs=out_specs, check_vma=False
    )
```

profile of v0, /device:TPU:102, one launch (start us, length us, event | category | flops | bytes accessed | tf_op | source)
XLA Modules:
  0.0 462.9 jit_solution(323516400858752026)
XLA Ops:
  12.8 76.4 %all-gather.3.cloned.1.call-done = bf16[8192,1,640]{2,0,1:T(8,128)(2,1)} async-done(((bf16[512,1,640]{2,0,1:T(8,128)(2,1)}), bf16[8192,1,640]{2,0,1:T(8,128)(2,1)}) %all-gather.3.cloned.1.call-update) | async-done | bytes 10485776 | tf_op jit(solution)/shard_map/all_gather | solution.py:31
  89.2 5.3 %fusion.97 = (bf16[8192,1,128]{2,0,1:T(8,128)(2,1)}, bf16[8192,1,128]{2,0,1:T(8,128)(2,1)}, bf16[8192,1,128]{2,0,1:T(8,128)(2,1)S(1)}) fusion(bf16[8192,1,640]{2,0,1:T(8,128)(2,1)} %all-gather.3.cloned.1.call-done), kind=kLoop, calls=%fused_computation.153 | loop fusion | bytes 12582912 | tf_op jit(solution)/shard_map/split | solution.py:31
  94.5 3.3 reshape.486
  97.8 10.6 %copy.25 = bf16[16,512,1,2,64]{1,4,3,2,0:T(8,128)(2,1)} copy(bf16[16,512,1,2,64]{4,3,1,0,2:T(2,128)(2,1)} %reshape.486) | data formatting | bytes 4194304 | tf_op jit(solution)/shard_map/while | solution.py:189
  108.4 4.7 %split.18 = bf16[8192,1,256]{2,0,1:T(8,128)(2,1)} slice(bf16[8192,1,640]{2,0,1:T(8,128)(2,1)} %all-gather.3.cloned.1.call-done), slice={[0:8192], [0:1], [128:384]} | slice | bytes 8388608 | tf_op jit(solution)/shard_map/split | solution.py:31
  113.0 6.9 %reshape.487 = bf16[16,512,1,2,128]{4,3,1,0,2:T(2,128)(2,1)} reshape(bf16[8192,1,256]{2,0,1:T(8,128)(2,1)} %split.18) | data formatting | bytes 8388608 | tf_op jit(solution)/shard_map/reshape | solution.py:163
  120.1 223.3 %while.32 = (s32[]{:T(128)}, f32[1,2,256]{2,1,0:T(2,128)S(1)}, f32[1,2,256]{2,1,0:T(2,128)S(1)}, f32[1,2,256,128]{3,2,1,0:T(8,128)S(1)}, f32[1,2,256]{2,1,0:T(2,...) while((s32[]{:T(128)}, f32[1,2,256]{2,1,0:T(2,128)S(1)}, ...), condition=%wide.region_13.14_spmd, body=%wide.region_0.13_spmd.sunk | while | flops 479992320 | bytes 19931888 | solution.py:189
  140.7 2.8 conditional.5
  154.7 2.8 conditional.5
  196.6 2.8 conditional.5
  210.5 2.8 conditional.5
  224.5 2.8 conditional.5
  238.4 2.8 conditional.5
  266.3 2.8 conditional.5
  280.3 2.8 conditional.5
  294.3 2.8 conditional.5
  322.2 2.8 conditional.5
  336.1 2.8 conditional.5
  346.5 31.3 %all_to_all.15 = bf16[8,64,2048]{2,1,0:T(8,128)(2,1)S(1)} all-to-all(bf16[8,64,2048]{2,1,0:T(8,128)(2,1)S(1)} %bitcast.192), channel_id=1, replica_groups=mesh['sp'=16,'tp'=8] {'tp'}, dimensions={0} | all-to-all | bytes 4194304 | tf_op jit(solution)/shard_map/all_to_all | solution.py:41
  381.0 3.8 all-to-all-start.1
  384.8 26.9 %all-to-all-done.1 = bf16[8,64,2048]{2,1,0:T(8,128)(2,1)S(1)} async-done(((bf16[8,64,2048]{2,1,0:T(8,128)(2,1)}), bf16[8,64,2048]{2,1,0:T(8,128)(2,1)S(1)}, u32[]{:S(2)}, u32[]{:S(2)}) %all-to-all-start.1) | async-done | bytes 2097184 | tf_op jit(solution)/shard_map/all_to_all | solution.py:53
  411.7 4.6 fusion.55
  416.3 7.9 %convolution_convert_fusion = bf16[512,2048]{1,0:T(8,128)(2,1)} fusion(bf16[2048,2112]{0,1:T(8,128)(2,1)} %all-gather.5.cloned.1.call-done, bf16[512,2048]{1,0:T(8,128)(2,1)S(1)} %bitcast.198, f32[512,704]{0,1:T(8,128)} %fusion.55), kind=kOutput, calls=%fused_computation.83 | convolution fusion | flops 2956001280 | bytes 11403264 | tf_op jit(solution)/shard_map/dot_general | solution.py:215
  424.2 30.7 %all_to_all.16 = bf16[8,64,2048]{2,1,0:T(8,128)(2,1)S(1)} all-to-all(bf16[8,64,2048]{2,1,0:T(8,128)(2,1)} %bitcast.199), channel_id=1, replica_groups=mesh['sp'=16,'tp'=8] {'tp'}, dimensions={0} | all-to-all | bytes 4194304 | tf_op jit(solution)/shard_map/all_to_all | solution.py:41
  (584 shorter events, 242.1 us)
Async XLA Ops:
  6.5 338.2 %copy-start = (bf16[128,2048]{1,0:T(8,128)(2,1)S(1)}, bf16[128,2048]{1,0:T(8,128)(2,1)}, u32[]{:S(2)}) copy-start(bf16[128,2048]{1,0:T(8,128)(2,1)} %param.32) | copy-start | bytes 1572868
  6.5 4.2 copy-start.3
  6.5 82.6 %all-gather.3.cloned.1.call-start = ((), (), s32[]{:S(2)}) async-start(), calls=%async_computation.3 | async-start | bytes 11141120 | tf_op jit(solution)/shard_map/all_gather | solution.py:31
  8.6 2.6 copy-start.4
  8.7 376.1 %all-gather.5.cloned.1.call-start = ((), (), s32[]{:S(2)}) async-start(), calls=%async_computation.4 | async-start | bytes 9191424 | tf_op jit(solution)/shard_map/all_gather | solution.py:17
  343.4 1.1 copy-start.6
  344.8 1.0 copy-start.2
  377.8 1.0 copy-start.1
  377.8 1.4 copy-start.5
  381.0 30.7 %all-to-all-start.1 = ((bf16[8,64,2048]{2,1,0:T(8,128)(2,1)}), bf16[8,64,2048]{2,1,0:T(8,128)(2,1)S(1)}, u32[]{:S(2)}, u32[]{:S(2)}) async-start(bf16[8,64,2048]{2,1,0:T(8,128)(2,1)} %broadcast_in_dim.48), calls=%async_computation.1 | async-start | bytes 4194304 | tf_op jit(solution)/shard_map/all_to_all | solution.py:53
Sparse Core Ops, SparseCore 0:
  9.5 79.6 all-gather.2
  91.3 77.8 all-gather.4
where the time goes:
time: 466 us; the launch traced here: 463 us
  local copies, waits for them, and re-layouts  119 us (26%)
  waiting for transfers between devices  103 us (22%)
  matrix products  70.2 us (15%)
  blocking collectives  62 us (13%)
  loops' own time  51.4 us (11%)
  other arithmetic  37.6 us (8%)
  between operations  15 us (3%)
    all_gather x1, waiting for transfers between devices, side_by_side(): lax.all_gather(both, axis, axis=dim, tiled=True)  76.4 us
    all_to_all x2, blocking collectives, sent_and_summed(): lax.all_to_all(split_up(array, dim, devices), axis, 0, 0, tiled=True)  62 us
    another operation x1, loops' own time, per_device(): lax.scan(step, (one_half, one_half), (jnp.arange(number, dtype=jnp.int32)...  49.6 us
    squeeze x32, local copies, waits for them, and re-layouts, per_device(): lax.scan(step, (one_half, one_half), (jnp.arange(number, dtype=jnp.int32)...  30.6 us
    dot_general x64, matrix products, absorb_group(): jnp.einsum('qhmd,khmd->hmqk', query_maps, key_block, preferred_element_ty...  28.5 us
    dynamic_slice x48, local copies, waits for them, and re-layouts, per_device(): lax.scan(step, (one_half, one_half), (jnp.arange(number, dtype=jnp.int32)...  28.4 us
    dot_general x64, matrix products, absorb_group(): jnp.einsum('hmqk,khe->hmqe', weights.astype(jnp.bfloat16), value_block, p...  27.8 us
    all_to_all x1, waiting for transfers between devices, from_everyone(): lax.all_to_all(jnp.broadcast_to(array[None], (devices, *array.shape)), ax...  26.9 us
  transfers between devices with their start and end apart: 3, of which 2 were waited for; matrix products, arithmetic and copies ran while one was open for 45% of the time, Pallas kernels for 0%

commit v1 on v0

v1 whole, which is shorter than its diff:
```python
import math

import jax
import jax.numpy as jnp
from jax import lax
from jax.experimental import pallas as pl
from jax.experimental.pallas import tpu as pltpu
from jax.sharding import PartitionSpec as P

residual_scale = 8.0**0.25
branch_scale = 0.8
norm_epsilon = 1e-05
masked_score = -1e30
log2e = math.log2(math.e)
MESH = pl.DeviceIdType.MESH
BF = jnp.bfloat16
F32 = jnp.float32
CH = 512


def remote(src, dst, ssem, rsem, sp, tp):
    return pltpu.make_async_remote_copy(
        src_ref=src, dst_ref=dst, send_sem=ssem, recv_sem=rsem, device_id=(sp, tp), device_id_type=MESH
    )


def attention_kernel(
    qs, ql, ks, kl, vs, vl, lam_in, gain, osm, ola, res, ngain,
    out,
    kv, qb, qz, lam, acc, mx, wo, ob, att, pre,
    q_ssem, q_rsem, x_ssem, kv_rsem, up_ssem, dn_ssem, pr_ssem,
    wu_ssem, wd_ssem, wp_ssem, w_rsem, o_ssem, o_rsem, l_sem,
):
    sp, tp = lax.axis_index("sp"), lax.axis_index("tp")
    z, x, y, c = sp // 4, sp % 4, tp // 2, tp % 2
    kind = x % 2
    large = kind == 1
    zu, zd, z2 = (z + 1) % 4, (z + 3) % 4, (z + 2) % 4
    yu, yd, y2 = (y + 1) % 4, (y + 3) % 4, (y + 2) % 4
    r = 2 * (3 - z) + c
    lo_chunk, hi_chunk = r, 15 - r

    def put(src, dst, ssem, rsem, dsp, dtp):
        same = jnp.logical_and(dsp == sp, dtp == tp)

        @pl.when(same)
        def _():
            pltpu.make_async_copy(src, dst, rsem).start()

        @pl.when(jnp.logical_not(same))
        def _():
            remote(src, dst, ssem, rsem, dsp, dtp).start()

    def put_done(src, dst, ssem, rsem, dsp, dtp):
        same = jnp.logical_and(dsp == sp, dtp == tp)

        @pl.when(jnp.logical_not(same))
        def _():
            remote(src, dst, ssem, rsem, dsp, dtp).wait_send()

    def got(dst, rsem):
        pltpu.make_async_copy(dst, dst, rsem).wait()

    dcore = 2 * y + x % 2
    small_sp, large_sp = 4 * z + 2 * c, 4 * z + 2 * c + 1
    kv_puts = [
        (ks, kv.at[sp, 0], x_ssem.at[0], kv_rsem.at[sp, 0], small_sp, dcore),
        (vs, kv.at[sp, 1], x_ssem.at[1], kv_rsem.at[sp, 1], small_sp, dcore),
        (kl.at[:, pl.ds(0, 128)], kv.at[sp, 0], x_ssem.at[2], kv_rsem.at[sp, 0], large_sp, dcore),
        (vl, kv.at[sp, 1], x_ssem.at[3], kv_rsem.at[sp, 1], large_sp, dcore),
        (kl.at[:, pl.ds(128, 128)], kv.at[sp, 2], x_ssem.at[4], kv_rsem.at[sp, 2], large_sp, dcore),
    ]
    low = jnp.minimum(sp, 15 - sp)
    hi = sp // 8
    qsp = 4 * (3 - low // 2) + 2 * c
    qtp = 2 * y + low % 2
    q_puts = [
        (qs, qb.at[hi, 0], q_ssem.at[0], q_rsem.at[hi, 0], qsp, qtp),
        (ql.at[:, pl.ds(0, 128)], qb.at[hi, 0], q_ssem.at[1], q_rsem.at[hi, 0], qsp + 1, qtp),
        (ql.at[:, pl.ds(128, 128)], qb.at[hi, 1], q_ssem.at[2], q_rsem.at[hi, 1], qsp + 1, qtp),
        (lam_in.at[0], lam.at[hi], q_ssem.at[3], q_rsem.at[hi, 2], qsp, qtp),
        (lam_in.at[1], lam.at[hi], q_ssem.at[4], q_rsem.at[hi, 2], qsp + 1, qtp),
    ]
    for p in kv_puts:
        put(*p)
    for p in q_puts:
        put(*p)

    wu, wd = 2 * yu + c, 2 * yd + c
    partner = 2 * y + 1 - c

    def w_send(slot, ssem, dtp, src=None):
        ref = wo.at[slot]
        return remote(ref if src is None else src, ref, ssem, w_rsem.at[slot], sp, dtp)

    own_a, own_b = tp, 8 + tp
    w_own = [
        w_send(own_a, wu_ssem.at[0], wu, osm), w_send(own_b, wd_ssem.at[0], wd, ola),
        w_send(own_b, wu_ssem.at[1], wu, ola), w_send(own_a, wd_ssem.at[1], wd, osm),
        w_send(own_a, wp_ssem.at[0], partner, osm), w_send(own_b, wp_ssem.at[1], partner, ola),
    ]
    for d in w_own:
        d.start()
    pltpu.make_async_copy(osm, wo.at[own_a], l_sem.at[0]).start()
    pltpu.make_async_copy(ola, wo.at[own_b], l_sem.at[1]).start()
    fwd_a, fwd_b = wd, 8 + wu
    w_f1 = [
        (fwd_a, w_send(fwd_a, wu_ssem.at[2], wu), w_send(fwd_a, wp_ssem.at[2], partner)),
        (fwd_b, w_send(fwd_b, wd_ssem.at[2], wd), w_send(fwd_b, wp_ssem.at[3], partner)),
    ]
    w_f2 = [
        (8 + wd, w_send(8 + wd, wp_ssem.at[4], partner)),
        (wu, w_send(wu, wp_ssem.at[5], partner)),
    ]
    w2 = 2 * y2 + c
    w_f3 = [
        (w2, w_send(w2, wp_ssem.at[6], partner)),
        (8 + w2, w_send(8 + w2, wp_ssem.at[7], partner)),
    ]

    def w_forward(items):
        for item in items:
            got(wo.at[item[0]], w_rsem.at[item[0]])
            for d in item[1:]:
                d.start()

    acc[...] = jnp.zeros_like(acc)
    mx[...] = jnp.full_like(mx, masked_score)

    for h in range(2):
        got(qb.at[h, 0], q_rsem.at[h, 0])
        got(lam.at[h], q_rsem.at[h, 2])

        @pl.when(large)
        def _():
            got(qb.at[h, 1], q_rsem.at[h, 1])
            qz[h, 0] = qb[h, 0]
            qz[h, 1] = qb[h, 1]

        @pl.when(jnp.logical_not(large))
        def _():
            both = qb[h, 0]
            first = lax.broadcasted_iota(jnp.int32, (CH, 128), 1) < 64
            qz[h, 0] = jnp.where(first, both, jnp.zeros_like(both))
            qz[h, 1] = jnp.where(first, jnp.zeros_like(both), both)

    factor = jnp.where(large, log2e * 128**-0.5, log2e * 64**-0.5).astype(F32)
    half = CH // 2

    def absorb(h, j, diagonal):
        values = jnp.concatenate([kv[j, 1], jnp.ones((CH, 128), BF)], axis=1)
        for m in range(2):
            keys = kv[j, 2 * m * kind]
            for t in range(2):
                rows = pl.ds(t * half, half)
                s = lax.dot_general(
                    qz[h, m, rows, :], keys, (((1,), (1,)), ((), ())), preferred_element_type=F32
                )
                if diagonal:
                    qi = lax.broadcasted_iota(jnp.int32, (half, CH), 0) + t * half
                    ki = lax.broadcasted_iota(jnp.int32, (half, CH), 1)
                    s = jnp.where(ki <= qi, s, masked_score)
                old = mx[h, m, rows, :]
                new = jnp.maximum(old, jnp.max(s, axis=1, keepdims=True))
                mx[h, m, rows, :] = new
                p = jnp.exp2((s - new[:, :1]) * factor)
                fade = jnp.exp2((old - new) * factor)
                pv = jnp.dot(p.astype(BF), values, preferred_element_type=F32)
                acc[h, m, rows, 0:128] = acc[h, m, rows, 0:128] * fade + pv[:, 0:128]
                acc[h, m, rows, 128:256] = acc[h, m, rows, 128:256] * fade + pv[:, 128:256]

    def kv_send(j, slab, ssem, dsp, dtp):
        return remote(kv.at[j, slab], kv.at[j, slab], ssem, kv_rsem.at[j, slab], dsp, dtp)

    def slabs(fn):
        fn(0)
        fn(1)

        @pl.when(large)
        def _():
            fn(2)

    def route(i):
        own = i < 2
        off = jnp.where(own, 0, jnp.where((i == 2) | (i == 4), 3, jnp.where(i < 6, 1, 2)))
        part = jnp.where((i == 0) | (i == 2) | (i == 5) | (i == 6), 0, 1)
        level = (z + off) % 4
        up = own | (i == 2)
        down = own | (i == 3)
        return level, part, up, down

    def kv_moves(i, act):
        level, part, up, down = route(i)
        j = 4 * level + 2 * part + c

        def one(s):
            @pl.when(up)
            def _():
                act(kv_send(j, s, up_ssem.at[jnp.minimum(i, 2), s], 4 * zu + x, tp))

            @pl.when(down)
            def _():
                act(kv_send(j, s, dn_ssem.at[jnp.minimum(i, 2), s], 4 * zd + x, tp))

            act(kv_send(j, s, pr_ssem.at[i, s], sp, partner))

        slabs(one)

    def phase(i, carry):
        level, part, up, down = route(i)
        first = 4 * level + 2 * part
        mine, other = first + c, first + 1 - c
        slabs(lambda s: got(kv.at[mine, s], kv_rsem.at[mine, s]))
        kv_moves(i, lambda d: d.start())

        @pl.when(i == 4)
        def _():
            w_forward(w_f1)

        @pl.when(i == 6)
        def _():
            w_forward(w_f2)

        slabs(lambda s: got(kv.at[other, s], kv_rsem.at[other, s]))
        n_lo = jnp.clip(lo_chunk - first + 1, 0, 2)
        n_hi = jnp.clip(hi_chunk - first + 1, 0, 2)

        def step(k, cc):
            h = jnp.where(k >= n_lo, 1, 0)
            j = first + k - h * n_lo
            diagonal = j == jnp.where(h == 1, hi_chunk, lo_chunk)

            @pl.when(diagonal)
            def _():
                absorb(h, j, True)

            @pl.when(jnp.logical_not(diagonal))
            def _():
                absorb(h, j, False)

            return cc

        lax.fori_loop(0, n_lo + n_hi, step, 0)
        return carry

    lax.fori_loop(0, 8, phase, 0)

    slot = 8 * kind + 2 * y + x // 2
    for h in range(2):
        for t in range(2):
            rows = pl.ds(t * half, half)
            one = acc[h, 0, rows, 0:128] / acc[h, 0, rows, 128:256]
            two = acc[h, 1, rows, 0:128] / acc[h, 1, rows, 128:256]
            combined = one - lam[h, 0:1, :] * two
            square = jnp.mean(combined * combined, axis=1, keepdims=True)
            normed = combined * lax.rsqrt(square + norm_epsilon) * gain[...] * branch_scale
            ob[h, rows, :] = normed.astype(BF)
        dsp = hi_chunk if h == 1 else lo_chunk
        for t in range(8):
            put(ob.at[h, pl.ds(64 * t, 64), :], att.at[slot], o_ssem.at[h, t], o_rsem.at[slot], dsp, t)

    w_forward(w_f3)
    pltpu.make_async_copy(osm, wo.at[own_a], l_sem.at[0]).wait()
    pltpu.make_async_copy(ola, wo.at[own_b], l_sem.at[1]).wait()
    for yy in (y, yu, yd, y2):
        for off in (0, 8):
            s = 2 * yy + 1 - c + off
            got(wo.at[s], w_rsem.at[s])
    for s in range(16):
        got(att.at[s], o_rsem.at[s])
    rows = jnp.concatenate([att[s] for s in range(16)], axis=1)

    def project(n, carry):
        cols = pl.ds(pl.multiple_of(n * 512, 512), 512)
        w = wo[:, :, cols].reshape(2048, 512)
        pre[:, cols] = residual_scale * res[:, cols].astype(F32) + jnp.dot(
            rows, w, preferred_element_type=F32
        )
        return carry

    lax.fori_loop(0, 4, project, 0)
    values = pre[...]
    centered = values - jnp.mean(values, axis=1, keepdims=True)
    variance = jnp.mean(centered * centered, axis=1, keepdims=True)
    out[...] = (centered * lax.rsqrt(variance + norm_epsilon) * ngain[...]).astype(BF)

    for p in kv_puts:
        put_done(*p)
    for p in q_puts:
        put_done(*p)
    for d in w_own:
        d.wait_send()
    for item in w_f1 + w_f2 + w_f3:
        for d in item[1:]:
            d.wait_send()

    def drain(i, carry):
        kv_moves(i, lambda d: d.wait_send())
        return carry

    lax.fori_loop(0, 8, drain, 0)
    for h in range(2):
        dsp = hi_chunk if h == 1 else lo_chunk
        for t in range(8):
            put_done(ob.at[h, pl.ds(64 * t, 64), :], att.at[slot], o_ssem.at[h, t], o_rsem.at[slot], dsp, t)


def attention(*args):
    dma = pltpu.SemaphoreType.DMA
    return pl.pallas_call(
        attention_kernel,
        name="attention",
        out_shape=jax.ShapeDtypeStruct((64, 2048), BF),
        in_specs=[pl.BlockSpec(memory_space=pltpu.VMEM)] * len(args),
        out_specs=pl.BlockSpec(memory_space=pltpu.VMEM),
        scratch_shapes=[
            pltpu.VMEM((16, 3, CH, 128), BF),
            pltpu.VMEM((2, 2, CH, 128), BF),
            pltpu.VMEM((2, 2, CH, 128), BF),
            pltpu.VMEM((2, 8, 128), F32),
            pltpu.VMEM((2, 2, CH, 256), F32),
            pltpu.VMEM((2, 2, CH, 128), F32),
            pltpu.VMEM((16, 128, 2048), BF),
            pltpu.VMEM((2, CH, 128), BF),
            pltpu.VMEM((16, 64, 128), BF),
            pltpu.VMEM((64, 2048), F32),
            dma((5,)), dma((2, 3)), dma((5,)), dma((16, 3)), dma((3, 3)), dma((3, 3)), dma((8, 3)),
            dma((3,)), dma((3,)), dma((8,)), dma((16,)), dma((2, 8)), dma((16,)), dma((2,)),
        ],
        compiler_params=pltpu.CompilerParams(has_side_effects=True, vmem_limit_bytes=60 * 1024 * 1024),
        cost_estimate=pl.CostEstimate(flops=8 * 10**9, bytes_accessed=10**8, transcendentals=10**7),
    )(*args)


def rows_first(arrays, axis, dims):
    turned = [jnp.moveaxis(a, dim, 0) for a, dim in zip(arrays, dims)]
    both = jnp.concatenate([t.reshape(len(t), -1) for t in turned], axis=1)
    whole, at, finished = (lax.all_gather(both, axis, axis=0, tiled=True), 0, [])
    for t, dim in zip(turned, dims):
        share = whole[:, at : at + t[0].size].reshape(-1, *t.shape[1:])
        finished.append(jnp.moveaxis(share, 0, dim))
        at += t[0].size
    return tuple(finished)


def split_up(array, dim, devices):
    before, after = (array.shape[:dim], array.shape[dim + 1 :])
    return jnp.moveaxis(array.reshape(*before, devices, -1, *after), dim, 0)


def sent_and_summed(array, axis, dim):
    devices = lax.axis_size(axis)
    tiles = lax.all_to_all(split_up(array, dim, devices), axis, 0, 0, tiled=True)
    return jnp.sum(tiles.astype(jnp.float32), axis=0)


def in_order(tiles, dim):
    dims = list(tiles.shape[1:])
    dims[dim] *= tiles.shape[0]
    return jnp.moveaxis(tiles, 0, dim).reshape(dims)


def from_everyone(array, axis):
    devices = lax.axis_size(axis)
    return lax.all_to_all(jnp.broadcast_to(array[None], (devices, *array.shape)), axis, 0, 0, tiled=True)


def per_device(
    residual, query_small, key_small, value_small, query_large, key_large, value_large,
    lambda_small, lambda_large, head_gain, output_small, output_large, norm_gain,
    gate_weight, up_weight, down_weight,
):
    gate_full, up_full, down_full = rows_first((gate_weight, up_weight, down_weight), "sp", (0, 0, 1))
    flat = lambda a: a.reshape(a.shape[0], a.shape[2])
    lam = jnp.broadcast_to(jnp.stack([lambda_small, lambda_large]).reshape(2, 1, 1), (2, 8, 128))
    normed = attention(
        flat(query_small), flat(query_large), flat(key_small), flat(key_large), flat(value_small),
        flat(value_large), lam, head_gain.reshape(1, 128), output_small, output_large, residual,
        norm_gain.reshape(1, 2048),
    )
    whole_rows = in_order(from_everyone(normed, "tp"), 0)
    gate_rows = jnp.dot(whole_rows, gate_full, preferred_element_type=jnp.float32)
    up_rows = jnp.dot(whole_rows, up_full, preferred_element_type=jnp.float32)
    hidden = (jax.nn.silu(gate_rows) * up_rows).astype(jnp.bfloat16)
    down_sum = sent_and_summed(
        jnp.dot(hidden, down_full, preferred_element_type=jnp.float32).astype(jnp.bfloat16), "tp", 0
    )
    return (residual_scale * normed.astype(jnp.float32) + 0.5 * down_sum).astype(jnp.bfloat16)


def solution(mesh):
    in_specs = (
        P(("sp", "tp"), None),
        P("sp", "tp", None), P("sp", "tp", None), P("sp", "tp", None),
        P("sp", "tp", None), P("sp", "tp", None), P("sp", "tp", None),
        P("tp"), P("tp"), P(), P("tp", None), P("tp", None), P(),
        P("sp", "tp"), P("sp", "tp"), P("tp", "sp"),
    )
    return jax.shard_map(
        per_device, mesh=mesh, in_specs=in_specs, out_specs=P(("sp", "tp"), None), check_vma=False
    )
```

time: 466 us -> 203 us (0.44)
  the two profiles are of different devices: /device:TPU:102 before, /device:TPU:96 now
where the time goes in v1:
time: 203 us; the launch traced here: 202 us
  Pallas kernels  107 us (53%)
  blocking collectives  63.8 us (31%)
  between operations  14.7 us (7%)
  matrix products  11 us (5%)
  other arithmetic  3.18 us (2%)
  local copies, waits for them, and re-layouts  2.45 us (1%)
    pallas_call x1, Pallas kernels, attention(): pl.pallas_call(attention_kernel, name='attention', out_shape=jax.ShapeDty...  107 us
    all_to_all x1, blocking collectives, from_everyone(): lax.all_to_all(jnp.broadcast_to(array[None], (devices, *array.shape)), ax...  33.1 us
    all_to_all x1, blocking collectives, sent_and_summed(): lax.all_to_all(split_up(array, dim, devices), axis, 0, 0, tiled=True)  30.7 us
    dot_general x1, matrix products, per_device(): jnp.dot(hidden, down_full, preferred_element_type=jnp.float32)  7.53 us
  transfers between devices with their start and end apart: 1, of which 0 were waited for; matrix products, arithmetic and copies ran while one was open for 1% of the time, Pallas kernels for 53%

profile of v1, /device:TPU:96, one launch (start us, length us, event | category | flops | bytes accessed | tf_op | source)
XLA Modules:
  0.0 202.4 jit_solution(4335685482728725920)
XLA Ops:
  6.5 0.0 all-gather.2.cloned.1.call-start
  6.5 2.0 pad_maximum_fusion
  8.5 0.0 all-gather.2.cloned.1.call-update
  9.8 0.1 maximum_bitcast_fusion
  9.9 0.7 broadcast_in_dim.14.lam_in
  10.6 107.3 %attention.1 = bf16[64,2048]{1,0:T(8,128)(2,1)} custom-call(bf16[512,128]{1,0:T(8,128)(2,1)} %bitcast.25, bf16[512,256]{1,0:T(8,128)(2,1)} %bitcast.23, bf16[512,128]{1,0:T(8,128)(2,1)} %bitcast.26, bf16[512,256]{1,0:T(8,128)(2,1)} %bitcast.24, bf16[512,128]{1,0:T(8,128)(2,1)} %bitcast.27, bf16[512,128]{1,0:T(8,128)(2,1)} %bitcast.28, ...), custom_call_target="tpu_custom_call" | custom-call | flops 8000000000 | bytes 100000000 | tf_op jit(solution)/shard_map/attention/pallas_call | solution.py:310
  117.8 1.2 broadcast_in_dim.15
  119.0 33.1 %all_to_all.10 = bf16[8,64,2048]{2,1,0:T(8,128)(2,1)S(1)} all-to-all(bf16[8,64,2048]{2,1,0:T(8,128)(2,1)S(1)} %broadcast_in_dim.15), channel_id=1, replica_groups=mesh['sp'=16,'tp'=8] {'tp'}, dimensions={0} | all-to-all | bytes 4194304 | tf_op jit(solution)/shard_map/all_to_all | solution.py:365
  152.1 0.0 all-gather.2.cloned.1.call-done
  152.1 3.5 %fusion.3 = f32[512,704]{0,1:T(8,128)S(1)} fusion(bf16[512,2048]{1,0:T(8,128)(2,1)S(1)} %bitcast.19, bf16[2048,2112]{0,1:T(8,128)(2,1)} %all-gather.2.cloned.1.call-done), kind=kOutput, calls=%fused_computation.5 | convolution fusion | flops 1476395008 | bytes 6422528 | tf_op jit(solution)/shard_map/dot_general | solution.py:382
  155.6 7.5 %convolution_convert_fusion = bf16[512,2048]{1,0:T(8,128)(2,1)} fusion(bf16[2048,2112]{0,1:T(8,128)(2,1)} %all-gather.2.cloned.1.call-done, bf16[512,2048]{1,0:T(8,128)(2,1)S(1)} %bitcast.20, f32[512,704]{0,1:T(8,128)S(1)} %fusion.3), kind=kOutput, calls=%fused_computation.1 | convolution fusion | flops 2956001280 | bytes 11403264 | tf_op jit(solution)/shard_map/dot_general | solution.py:386
  163.1 30.7 %all_to_all.11 = bf16[8,64,2048]{2,1,0:T(8,128)(2,1)S(1)} all-to-all(bf16[8,64,2048]{2,1,0:T(8,128)(2,1)} %bitcast.21), channel_id=1, replica_groups=mesh['sp'=16,'tp'=8] {'tp'}, dimensions={0} | all-to-all | bytes 4194304 | tf_op jit(solution)/shard_map/all_to_all | solution.py:353
  193.9 0.0 copy-start
  193.9 0.4 convert_reduce_fusion
  194.2 0.6 copy-done
  194.8 0.8 add_convert_fusion
Async XLA Ops:
  6.5 145.6 %all-gather.2.cloned.1.call-start = ((), (), s32[]{:S(2)}) async-start(), calls=%async_computation.2 | async-start | bytes 9191424 | tf_op jit(solution)/shard_map/all_gather | solution.py:338
  193.9 1.0 copy-start
Sparse Core Ops, SparseCore 0:
  9.4 104.6 all-gather.1

commit v2 on v1

--- a/solution.py
+++ b/solution.py
@@ -24,12 +24,13 @@
     )
 
 
-def attention_kernel(
-    qs, ql, ks, kl, vs, vl, lam_in, gain, osm, ola, res, ngain,
+def block_kernel(
+    qs, ql, ks, kl, vs, vl, lam_in, gain, osm, ola, res, ngain, gw, uw, dw,
     out,
-    kv, qb, qz, lam, acc, mx, wo, ob, att, pre,
+    kv, qb, qz, lam, acc, mx, wo, ob, att, pre, wt, nb, psend, precv, mine_f, rsend, rrecv, tbuf,
     q_ssem, q_rsem, x_ssem, kv_rsem, up_ssem, dn_ssem, pr_ssem,
     wu_ssem, wd_ssem, wp_ssem, w_rsem, o_ssem, o_rsem, l_sem,
+    g_ssem, g_rsem, nu_ssem, nd_ssem, np_ssem, n_rsem, p_ssem, p_rsem, r_ssem, r_rsem, t_rsem,
 ):
     sp, tp = lax.axis_index("sp"), lax.axis_index("tp")
     z, x, y, c = sp // 4, sp % 4, tp // 2, tp % 2
@@ -37,6 +38,7 @@
     large = kind == 1
     zu, zd, z2 = (z + 1) % 4, (z + 3) % 4, (z + 2) % 4
     yu, yd, y2 = (y + 1) % 4, (y + 3) % 4, (y + 2) % 4
+    xu, xd, x2 = (x + 1) % 4, (x + 3) % 4, (x + 2) % 4
     r = 2 * (3 - z) + c
     lo_chunk, hi_chunk = r, 15 - r
 
@@ -85,6 +87,70 @@
         put(*p)
     for p in q_puts:
         put(*p)
+
+    own_piece = (gw, uw, dw.at[pl.ds(0, 352), :], dw.at[pl.ds(352, 352), :])
+
+    def piece(s, k):
+        return wt.at[s, k] if k < 2 else wt.at[s, 2, pl.ds(352 * (k - 2), 352), :]
+
+    class Ring:
+        def __init__(self, at, along_x, first, line):
+            self.at, self.first = at, first
+            if along_x:
+                self.slots = [4 * line + p for p in (x, xd, xu, x2)]
+                self.up, self.down = 4 * z + xu, 4 * z + xd
+            else:
+                self.slots = [4 * p + line for p in (z, zd, zu, z2)]
+                self.up, self.down = 4 * zu + x, 4 * zd + x
+
+        def send(self, n, which, k, to, src=None):
+            s = self.slots[which]
+            ref = piece(s, k)
+            return remote(ref if src is None else src, ref, g_ssem.at[self.at, n], g_rsem.at[s, k], to, tp)
+
+        def own_sends(self, from_input=False):
+            a, b = self.first, self.first + 1
+            sa, sb = (own_piece[a], own_piece[b]) if from_input else (None, None)
+            return [
+                self.send(0, 0, a, self.up, sa), self.send(1, 0, b, self.down, sb),
+                self.send(2, 0, b, self.up, sb), self.send(3, 0, a, self.down, sa),
+            ]
+
+        def far_sends(self):
+            return self.send(4, 1, self.first, self.up), self.send(5, 2, self.first + 1, self.down)
+
+        def got(self, which, k):
+            got(piece(self.slots[which], k), g_rsem.at[self.slots[which], k])
+
+        def own(self, from_input=False):
+            for d in self.own_sends(from_input):
+                d.start()
+
+        def forward(self):
+            f1, f2 = self.far_sends()
+            self.got(1, self.first)
+            f1.start()
+            self.got(2, self.first + 1)
+            f2.start()
+
+        def near(self):
+            self.got(1, self.first + 1)
+            self.got(2, self.first)
+
+        def far(self):
+            self.got(3, self.first)
+            self.got(3, self.first + 1)
+
+        def drain(self):
+            for d in (*self.own_sends(), *self.far_sends()):
+                d.wait_send()
+
+    r0 = Ring(0, False, 0, x)
+    r1, r2, r3, r4 = [Ring(1 + n, True, 0, line) for n, line in enumerate((z, zd, zu, z2))]
+    r5 = Ring(5, True, 2, z)
+    r6, r7, r8, r9 = [Ring(6 + n, False, 2, line) for n, line in enumerate((x, xd, xu, x2))]
+    for ring in (r0, r1, r5, r6):
+        ring.own(True)
 
     wu, wd = 2 * yu + c, 2 * yd + c
     partner = 2 * y + 1 - c
@@ -210,6 +276,29 @@
         level, part, up, down = route(i)
         first = 4 * level + 2 * part
         mine, other = first + c, first + 1 - c
+
+        @pl.when(i == 2)
+        def _():
+            r0.forward()
+            r0.near()
+            r2.own()
+            r3.own()
+
+        @pl.when(i == 4)
+        def _():
+            r1.forward()
+            r5.forward()
+            r5.near()
+            r7.own()
+            r8.own()
+
+        @pl.when(i == 6)
+        def _():
+            r0.far()
+            r4.own()
+            r5.far()
+            r9.own()
+
         slabs(lambda s: got(kv.at[mine, s], kv_rsem.at[mine, s]))
         kv_moves(i, lambda d: d.start())
 
@@ -259,6 +348,11 @@
         for t in range(8):
             put(ob.at[h, pl.ds(64 * t, 64), :], att.at[slot], o_ssem.at[h, t], o_rsem.at[slot], dsp, t)
 
+    r2.forward()
+    r3.forward()
+    r6.forward()
+    r7.forward()
+    r8.forward()
     w_forward(w_f3)
     pltpu.make_async_copy(osm, wo.at[own_a], l_sem.at[0]).wait()
     pltpu.make_async_copy(ola, wo.at[own_b], l_sem.at[1]).wait()
@@ -282,7 +376,108 @@
     values = pre[...]
     centered = values - jnp.mean(values, axis=1, keepdims=True)
     variance = jnp.mean(centered * centered, axis=1, keepdims=True)
-    out[...] = (centered * lax.rsqrt(variance + norm_epsilon) * ngain[...]).astype(BF)
+    normed = (centered * lax.rsqrt(variance + norm_epsilon) * ngain[...]).astype(BF)
+    nb[tp, 0] = normed[:, 0:1024]
+    nb[tp, 1] = normed[:, 1024:2048]
+
+    def n_send(t, k, ssem, dtp):
+        return remote(nb.at[t, k], nb.at[t, k], ssem, n_rsem.at[t, k], sp, dtp)
+
+    n_own = [
+        n_send(tp, 0, nu_ssem.at[0], wu), n_send(tp, 1, nd_ssem.at[0], wd),
+        n_send(tp, 1, nu_ssem.at[1], wu), n_send(tp, 0, nd_ssem.at[1], wd),
+        n_send(tp, 0, np_ssem.at[0], partner), n_send(tp, 1, np_ssem.at[1], partner),
+    ]
+    n_fwd = [
+        (wd, 0, [n_send(wd, 0, nu_ssem.at[2], wu), n_send(wd, 0, np_ssem.at[2], partner)]),
+        (wu, 1, [n_send(wu, 1, nd_ssem.at[2], wd), n_send(wu, 1, np_ssem.at[3], partner)]),
+        (wd, 1, [n_send(wd, 1, np_ssem.at[4], partner)]),
+        (wu, 0, [n_send(wu, 0, np_ssem.at[5], partner)]),
+        (w2, 0, [n_send(w2, 0, np_ssem.at[6], partner)]),
+        (w2, 1, [n_send(w2, 1, np_ssem.at[7], partner)]),
+    ]
+    for d in n_own:
+        d.start()
+    r4.forward()
+    r9.forward()
+    for t, k, sends in n_fwd:
+        got(nb.at[t, k], n_rsem.at[t, k])
+        for d in sends:
+            d.start()
+    wt[sp, 0] = gw[...]
+    wt[sp, 1] = uw[...]
+    wt[sp, 2] = dw[...]
+    for ring in (r1, r2, r3, r4, r6, r7, r8, r9):
+        ring.near()
+        ring.far()
+
+    def mixer(groups):
+        rows = []
+        for g, yy in groups:
+            t = 2 * yy + 1 - c
+            got(nb.at[t, 0], n_rsem.at[t, 0])
+            got(nb.at[t, 1], n_rsem.at[t, 1])
+            for t in (2 * yy + 1 - c, 2 * yy + c):
+                rows.append(jnp.concatenate([nb[t, 0], nb[t, 1]], axis=1))
+        rows = jnp.concatenate(rows, axis=0)
+        nt = (((1,), (1,)), ((), ()))
+        gate = lax.dot_general(
+            rows, jnp.concatenate([wt[s, 0] for s in range(16)], axis=1), nt, preferred_element_type=F32
+        )
+        up = lax.dot_general(
+            rows, jnp.concatenate([wt[s, 1] for s in range(16)], axis=1), nt, preferred_element_type=F32
+        )
+        hidden = (gate / (1.0 + jnp.exp(-gate)) * up).astype(BF)
+        for n in range(8):
+            cols = pl.ds(256 * n, 256)
+            w = jnp.concatenate([wt[2 * n, 2], wt[2 * n + 1, 2]], axis=1)
+            part = jnp.dot(hidden, w, preferred_element_type=F32)
+            for at, (g, yy) in enumerate(groups):
+                psend[g, :, cols] = part[128 * at : 128 * at + 64].astype(BF)
+                mine_f[g, :, cols] = part[128 * at + 64 : 128 * at + 128]
+        for g, yy in groups:
+            p_move(g).start()
+
+    def p_move(g):
+        return remote(psend.at[g], precv.at[g], p_ssem.at[g], p_rsem.at[g], sp, partner)
+
+    def pair_sum(g):
+        got(precv.at[g], p_rsem.at[g])
+        both = (mine_f[g] + precv[g].astype(F32)).astype(BF)
+        rsend[g, 0] = both[:, 0:1024]
+        rsend[g, 1] = both[:, 1024:2048]
+
+    r_up = remote(rsend.at[1], rrecv.at[0], r_ssem.at[0], r_rsem.at[0], sp, wu)
+    r_down = remote(rsend.at[2], rrecv.at[1], r_ssem.at[1], r_rsem.at[1], sp, wd)
+    r_a = remote(rsend.at[0, 0], tbuf.at[0], r_ssem.at[2], t_rsem.at[0], sp, wu)
+    r_b = remote(rsend.at[0, 1], tbuf.at[1], r_ssem.at[3], t_rsem.at[1], sp, wd)
+    f_a = remote(tbuf.at[0], rrecv.at[2, 0], r_ssem.at[4], r_rsem.at[2], sp, wu)
+    f_b = remote(tbuf.at[1], rrecv.at[2, 1], r_ssem.at[5], r_rsem.at[3], sp, wd)
+    mixer([(0, y2)])
+    pair_sum(0)
+    r_a.start()
+    r_b.start()
+    mixer([(1, yu), (2, yd)])
+    got(tbuf.at[0], t_rsem.at[0])
+    f_a.start()
+    got(tbuf.at[1], t_rsem.at[1])
+    f_b.start()
+    pair_sum(1)
+    r_up.start()
+    pair_sum(2)
+    r_down.start()
+    mixer_own = [(3, y)]
+    mixer(mixer_own)
+    got(precv.at[3], p_rsem.at[3])
+    pre[...] = residual_scale * normed.astype(F32) + 0.5 * (mine_f[3] + precv[3].astype(F32))
+    got(rrecv.at[0], r_rsem.at[0])
+    got(rrecv.at[1], r_rsem.at[1])
+    got(rrecv.at[2, 0], r_rsem.at[2])
+    got(rrecv.at[2, 1], r_rsem.at[3])
+    for k in range(2):
+        cols = pl.ds(1024 * k, 1024)
+        more = rrecv[0, k].astype(F32) + rrecv[1, k].astype(F32) + rrecv[2, k].astype(F32)
+        out[:, cols] = (pre[:, cols] + 0.5 * more).astype(BF)
 
     for p in kv_puts:
         put_done(*p)
@@ -294,6 +489,18 @@
         for d in item[1:]:
             d.wait_send()
 
+    for ring in (r0, r1, r2, r3, r4, r5, r6, r7, r8, r9):
+        ring.drain()
+    for d in n_own:
+        d.wait_send()
+    for t, k, sends in n_fwd:
+        for d in sends:
+            d.wait_send()
+    for g in range(4):
+        p_move(g).wait_send()
+    for d in (r_up, r_down, r_a, r_b, f_a, f_b):
+        d.wait_send()
+
     def drain(i, carry):
         kv_moves(i, lambda d: d.wait_send())
         return carry
@@ -305,11 +512,11 @@
             put_done(ob.at[h, pl.ds(64 * t, 64), :], att.at[slot], o_ssem.at[h, t], o_rsem.at[slot], dsp, t)
 
 
-def attention(*args):
+def block(*args):
     dma = pltpu.SemaphoreType.DMA
     return pl.pallas_call(
-        attention_kernel,
-        name="attention",
+        block_kernel,
+        name="block",
         out_shape=jax.ShapeDtypeStruct((64, 2048), BF),
         in_specs=[pl.BlockSpec(memory_space=pltpu.VMEM)] * len(args),
         out_specs=pl.BlockSpec(memory_space=pltpu.VMEM),
@@ -324,45 +531,22 @@
             pltpu.VMEM((2, CH, 128), BF),
             pltpu.VMEM((16, 64, 128), BF),
             pltpu.VMEM((64, 2048), F32),
+            pltpu.VMEM((16, 3, 704, 128), BF),
+            pltpu.VMEM((8, 2, 64, 1024), BF),
+            pltpu.VMEM((4, 64, 2048), BF),
+            pltpu.VMEM((4, 64, 2048), BF),
+            pltpu.VMEM((4, 64, 2048), F32),
+            pltpu.VMEM((3, 2, 64, 1024), BF),
+            pltpu.VMEM((3, 2, 64, 1024), BF),
+            pltpu.VMEM((2, 64, 1024), BF),
             dma((5,)), dma((2, 3)), dma((5,)), dma((16, 3)), dma((3, 3)), dma((3, 3)), dma((8, 3)),
             dma((3,)), dma((3,)), dma((8,)), dma((16,)), dma((2, 8)), dma((16,)), dma((2,)),
+            dma((10, 6)), dma((16, 4)), dma((3,)), dma((3,)), dma((8,)), dma((8, 2)),
+            dma((4,)), dma((4,)), dma((6,)), dma((4,)), dma((2,)),
         ],
         compiler_params=pltpu.CompilerParams(has_side_effects=True, vmem_limit_bytes=60 * 1024 * 1024),
         cost_estimate=pl.CostEstimate(flops=8 * 10**9, bytes_accessed=10**8, transcendentals=10**7),
     )(*args)
-
-
-def rows_first(arrays, axis, dims):
-    turned = [jnp.moveaxis(a, dim, 0) for a, dim in zip(arrays, dims)]
-    both = jnp.concatenate([t.reshape(len(t), -1) for t in turned], axis=1)
-    whole, at, finished = (lax.all_gather(both, axis, axis=0, tiled=True), 0, [])
-    for t, dim in zip(turned, dims):
-        share = whole[:, at : at + t[0].size].reshape(-1, *t.shape[1:])
-        finished.append(jnp.moveaxis(share, 0, dim))
-        at += t[0].size
-    return tuple(finished)
-
-
-def split_up(array, dim, devices):
-    before, after = (array.shape[:dim], array.shape[dim + 1 :])
-    return jnp.moveaxis(array.reshape(*before, devices, -1, *after), dim, 0)
-
-
-def sent_and_summed(array, axis, dim):
-    devices = lax.axis_size(axis)
-    tiles = lax.all_to_all(split_up(array, dim, devices), axis, 0, 0, tiled=True)
-    return jnp.sum(tiles.astype(jnp.float32), axis=0)
-
-
-def in_order(tiles, dim):
-    dims = list(tiles.shape[1:])
-    dims[dim] *= tiles.shape[0]
-    return jnp.moveaxis(tiles, 0, dim).reshape(dims)
-
-
-def from_everyone(array, axis):
-    devices = lax.axis_size(axis)
-    return lax.all_to_all(jnp.broadcast_to(array[None], (devices, *array.shape)), axis, 0, 0, tiled=True)
 
 
 def per_device(
@@ -370,22 +554,13 @@
     lambda_small, lambda_large, head_gain, output_small, output_large, norm_gain,
     gate_weight, up_weight, down_weight,
 ):
-    gate_full, up_full, down_full = rows_first((gate_weight, up_weight, down_weight), "sp", (0, 0, 1))
     flat = lambda a: a.reshape(a.shape[0], a.shape[2])
     lam = jnp.broadcast_to(jnp.stack([lambda_small, lambda_large]).reshape(2, 1, 1), (2, 8, 128))
-    normed = attention(
+    return block(
         flat(query_small), flat(query_large), flat(key_small), flat(key_large), flat(value_small),
         flat(value_large), lam, head_gain.reshape(1, 128), output_small, output_large, residual,
-        norm_gain.reshape(1, 2048),
+        norm_gain.reshape(1, 2048), gate_weight.T, up_weight.T, down_weight,
     )
-    whole_rows = in_order(from_everyone(normed, "tp"), 0)
-    gate_rows = jnp.dot(whole_rows, gate_full, preferred_element_type=jnp.float32)
-    up_rows = jnp.dot(whole_rows, up_full, preferred_element_type=jnp.float32)
-    hidden = (jax.nn.silu(gate_rows) * up_rows).astype(jnp.bfloat16)
-    down_sum = sent_and_summed(
-        jnp.dot(hidden, down_full, preferred_element_type=jnp.float32).astype(jnp.bfloat16), "tp", 0
-    )
-    return (residual_scale * normed.astype(jnp.float32) + 0.5 * down_sum).astype(jnp.bfloat16)
 
 
 def solution(mesh):

time: 203 us -> 130 us (0.64)
  blocking collectives: 63.8 us -> 0 us
  Pallas kernels: 107 us -> 126 us
  between operations: 14.7 us -> 1.31 us
  matrix products: 11 us -> 0 us
  other arithmetic: 3.18 us -> 0.07 us
    all_to_all x2 -> x0, blocking collectives: 63.8 us -> none  [the longest x1 33.1 us: from_everyone(): lax.all_to_all(jnp.broadcast_to(array[None], (devices, *array.shape)), ax...]
    pallas_call x1, Pallas kernels: 107 us -> 126 us  [block(): pl.pallas_call(block_kernel, name='block', out_shape=jax.ShapeDtypeStruct...]
    dot_general x2 -> x0, matrix products: 11 us -> none  [the longest x1 7.53 us: per_device(): jnp.dot(hidden, down_full, preferred_element_type=jnp.float32)]
  transfers between devices with their start and end apart: 1 -> 0, of which waited for: 0 -> 0; matrix products, arithmetic and copies ran while one was open for 1% -> 0% of each run, Pallas kernels for 53% -> 0%
where the time goes in v2:
time: 130 us
  Pallas kernels  126 us (97%)
  local copies, waits for them, and re-layouts  2.34 us (2%)
  between operations  1.31 us (1%)
    pallas_call x1, Pallas kernels, block(): pl.pallas_call(block_kernel, name='block', out_shape=jax.ShapeDtypeStruct...  126 us

profile of v2, /device:TPU:96, one launch (start us, length us, event | category | flops | bytes accessed | tf_op | source)
XLA Modules:
  0.0 129.9 jit_solution(8651381084402118309)
XLA Ops:
  1.3 0.1 maximum_bitcast_fusion
  1.4 0.7 broadcast_in_dim.8.lam_in
  2.0 126.1 %block.1 = bf16[64,2048]{1,0:T(8,128)(2,1)} custom-call(bf16[512,128]{1,0:T(8,128)(2,1)} %bitcast.20, bf16[512,256]{1,0:T(8,128)(2,1)} %bitcast.16, bf16[512,128]{1,0:T(8,128)(2,1)} %bitcast.21, bf16[512,256]{1,0:T(8,128)(2,1)} %bitcast.17, bf16[512,128]{1,0:T(8,128)(2,1)} %bitcast.22, bf16[512,128]{1,0:T(8,128)(2,1)} %bitcast.23, ...), custom_call_target="tpu_custom_call" | custom-call | flops 8000000000 | bytes 100000000 | tf_op jit(solution)/shard_map/block/pallas_call | solution.py:517
  128.2 1.7 %copy.20 = bf16[64,2048]{1,0:T(8,128)(2,1)} copy(bf16[64,2048]{1,0:T(8,128)(2,1)} %block.1) | data formatting | bytes 524288

commit v3 on v2

--- a/solution.py
+++ b/solution.py
@@ -25,12 +25,12 @@
 
 
 def block_kernel(
-    qs, ql, ks, kl, vs, vl, lam_in, gain, osm, ola, res, ngain, gw, uw, dw,
+    qs_in, ql_in, ks_in, kl_in, vs_in, vl_in, lam_in, gain, osm, ola, res, ngain, gw, uw, dw,
     out,
-    kv, qb, qz, lam, acc, mx, wo, ob, att, pre, wt, nb, psend, precv, mine_f, rsend, rrecv, tbuf,
+    qs, ql, ks, kl, vs, vl, kv, qb, qz, lam, acc, mx, wo, ob, att, pre, wt, nb, psend, precv, mine_f, rsend, rrecv, tbuf,
     q_ssem, q_rsem, x_ssem, kv_rsem, up_ssem, dn_ssem, pr_ssem,
     wu_ssem, wd_ssem, wp_ssem, w_rsem, o_ssem, o_rsem, l_sem,
-    g_ssem, g_rsem, nu_ssem, nd_ssem, np_ssem, n_rsem, p_ssem, p_rsem, r_ssem, r_rsem, t_rsem,
+    g_ssem, g_rsem, nu_ssem, nd_ssem, np_ssem, n_rsem, p_ssem, p_rsem, r_ssem, r_rsem, t_rsem, i_sem,
 ):
     sp, tp = lax.axis_index("sp"), lax.axis_index("tp")
     z, x, y, c = sp // 4, sp % 4, tp // 2, tp % 2
@@ -63,6 +63,14 @@
     def got(dst, rsem):
         pltpu.make_async_copy(dst, dst, rsem).wait()
 
+    staged = [
+        pltpu.make_async_copy(a, b, i_sem.at[n])
+        for n, (a, b) in enumerate(
+            ((ks_in, ks), (vs_in, vs), (kl_in, kl), (vl_in, vl), (qs_in, qs), (ql_in, ql))
+        )
+    ]
+    for d in staged:
+        d.start()
     dcore = 2 * y + x % 2
     small_sp, large_sp = 4 * z + 2 * c, 4 * z + 2 * c + 1
     kv_puts = [
@@ -83,8 +91,34 @@
         (lam_in.at[0], lam.at[hi], q_ssem.at[3], q_rsem.at[hi, 2], qsp, qtp),
         (lam_in.at[1], lam.at[hi], q_ssem.at[4], q_rsem.at[hi, 2], qsp + 1, qtp),
     ]
-    for p in kv_puts:
-        put(*p)
+    barrier = pltpu.get_barrier_semaphore()
+
+    def greet(dsp, dtp):
+        @pl.when(jnp.logical_not(jnp.logical_and(dsp == sp, dtp == tp)))
+        def _():
+            pl.semaphore_signal(barrier, inc=1, device_id=(dsp, dtp), device_id_type=MESH)
+
+    sources = [(4 * z + c, 2 * y + x // 2), (4 * z + c + 2, 2 * y + x // 2)]
+    targets = [(small_sp, dcore), (large_sp, dcore)]
+    sources += [(lo_chunk, 2 * y + x // 2), (hi_chunk, 2 * y + x // 2)]
+    targets += [(qsp, qtp), (qsp + 1, qtp)]
+    near = [(4 * zu + x, tp), (4 * zd + x, tp), (4 * z + xu, tp), (4 * z + xd, tp)]
+    near += [(sp, 2 * yu + c), (sp, 2 * yd + c), (sp, 2 * y + 1 - c)]
+    sources += near + [(4 * (3 - low // 2) + a, 2 * b + low % 2) for a in range(4) for b in range(4)]
+    targets += near + [(a, t) for a in (lo_chunk, hi_chunk) for t in range(8)]
+    for d in sources:
+        greet(*d)
+    count = len(targets)
+    for d in targets:
+        count -= jnp.logical_and(d[0] == sp, d[1] == tp).astype(jnp.int32)
+    with jax.named_scope("barrier"):
+        pl.semaphore_wait(barrier, count)
+    for d, p in zip(staged, (kv_puts[:1], kv_puts[1:2], kv_puts[2:3] + kv_puts[4:], kv_puts[3:4])):
+        d.wait()
+        for one in p:
+            put(*one)
+    for d in staged[4:]:
+        d.wait()
     for p in q_puts:
         put(*p)
 
@@ -149,7 +183,7 @@
     r1, r2, r3, r4 = [Ring(1 + n, True, 0, line) for n, line in enumerate((z, zd, zu, z2))]
     r5 = Ring(5, True, 2, z)
     r6, r7, r8, r9 = [Ring(6 + n, False, 2, line) for n, line in enumerate((x, xd, xu, x2))]
-    for ring in (r0, r1, r5, r6):
+    for ring in (r0, r1, r5):
         ring.own(True)
 
     wu, wd = 2 * yu + c, 2 * yd + c
@@ -190,25 +224,10 @@
             for d in item[1:]:
                 d.start()
 
+    for n, a in enumerate((gw, uw, dw)):
+        pltpu.make_async_copy(a, wt.at[sp, n], i_sem.at[6 + n]).start()
     acc[...] = jnp.zeros_like(acc)
     mx[...] = jnp.full_like(mx, masked_score)
-
-    for h in range(2):
-        got(qb.at[h, 0], q_rsem.at[h, 0])
-        got(lam.at[h], q_rsem.at[h, 2])
-
-        @pl.when(large)
-        def _():
-            got(qb.at[h, 1], q_rsem.at[h, 1])
-            qz[h, 0] = qb[h, 0]
-            qz[h, 1] = qb[h, 1]
-
-        @pl.when(jnp.logical_not(large))
-        def _():
-            both = qb[h, 0]
-            first = lax.broadcasted_iota(jnp.int32, (CH, 128), 1) < 64
-            qz[h, 0] = jnp.where(first, both, jnp.zeros_like(both))
-            qz[h, 1] = jnp.where(first, jnp.zeros_like(both), both)
 
     factor = jnp.where(large, log2e * 128**-0.5, log2e * 64**-0.5).astype(F32)
     half = CH // 2
@@ -272,45 +291,71 @@
 
         slabs(one)
 
+    def kv_arrive(i):
+        level, part, up, down = route(i)
+        mine = 4 * level + 2 * part + c
+        with jax.named_scope("wait_kv"):
+            slabs(lambda s: got(kv.at[mine, s], kv_rsem.at[mine, s]))
+        kv_moves(i, lambda d: d.start())
+
+    kv_arrive(0)
+    kv_arrive(1)
+    with jax.named_scope("ev_pre"):
+        r0.forward()
+        r0.near()
+        r2.own()
+        r3.own()
+        r6.own(True)
+    with jax.named_scope("wait_q"):
+        for h in range(2):
+            got(qb.at[h, 0], q_rsem.at[h, 0])
+            got(lam.at[h], q_rsem.at[h, 2])
+
+            @pl.when(large)
+            def _():
+                got(qb.at[h, 1], q_rsem.at[h, 1])
+                qz[h, 0] = qb[h, 0]
+                qz[h, 1] = qb[h, 1]
+
+            @pl.when(jnp.logical_not(large))
+            def _():
+                both = qb[h, 0]
+                first = lax.broadcasted_iota(jnp.int32, (CH, 128), 1) < 64
+                qz[h, 0] = jnp.where(first, both, jnp.zeros_like(both))
+                qz[h, 1] = jnp.where(first, jnp.zeros_like(both), both)
+
     def phase(i, carry):
         level, part, up, down = route(i)
         first = 4 * level + 2 * part
-        mine, other = first + c, first + 1 - c
-
-        @pl.when(i == 2)
+        other = first + 1 - c
+
+        @pl.when(i >= 2)
         def _():
-            r0.forward()
-            r0.near()
-            r2.own()
-            r3.own()
-
-        @pl.when(i == 4)
-        def _():
-            r1.forward()
-            r5.forward()
-            r5.near()
-            r7.own()
-            r8.own()
-
-        @pl.when(i == 6)
-        def _():
-            r0.far()
-            r4.own()
-            r5.far()
-            r9.own()
-
-        slabs(lambda s: got(kv.at[mine, s], kv_rsem.at[mine, s]))
-        kv_moves(i, lambda d: d.start())
-
-        @pl.when(i == 4)
-        def _():
-            w_forward(w_f1)
-
-        @pl.when(i == 6)
-        def _():
-            w_forward(w_f2)
-
-        slabs(lambda s: got(kv.at[other, s], kv_rsem.at[other, s]))
+            kv_arrive(i)
+
+        with jax.named_scope("ev_w"):
+            @pl.when(i == 2)
+            def _():
+                r1.forward()
+
+            @pl.when(i == 4)
+            def _():
+                r5.forward()
+                r5.near()
+                r7.own()
+                r8.own()
+                r0.far()
+                r4.own()
+                w_forward(w_f1)
+
+            @pl.when(i == 6)
+            def _():
+                r2.forward()
+                r3.forward()
+                w_forward(w_f2)
+
+        with jax.named_scope("wait_kv2"):
+            slabs(lambda s: got(kv.at[other, s], kv_rsem.at[other, s]))
         n_lo = jnp.clip(lo_chunk - first + 1, 0, 2)
         n_hi = jnp.clip(hi_chunk - first + 1, 0, 2)
 
@@ -329,7 +374,8 @@
 
             return cc
 
-        lax.fori_loop(0, n_lo + n_hi, step, 0)
+        with jax.named_scope("attn"):
+            lax.fori_loop(0, n_lo + n_hi, step, 0)
         return carry
 
     lax.fori_loop(0, 8, phase, 0)
@@ -348,20 +394,24 @@
         for t in range(8):
             put(ob.at[h, pl.ds(64 * t, 64), :], att.at[slot], o_ssem.at[h, t], o_rsem.at[slot], dsp, t)
 
-    r2.forward()
-    r3.forward()
-    r6.forward()
-    r7.forward()
-    r8.forward()
-    w_forward(w_f3)
-    pltpu.make_async_copy(osm, wo.at[own_a], l_sem.at[0]).wait()
-    pltpu.make_async_copy(ola, wo.at[own_b], l_sem.at[1]).wait()
-    for yy in (y, yu, yd, y2):
-        for off in (0, 8):
-            s = 2 * yy + 1 - c + off
-            got(wo.at[s], w_rsem.at[s])
-    for s in range(16):
-        got(att.at[s], o_rsem.at[s])
+    with jax.named_scope("ev_post"):
+        r6.forward()
+        r7.forward()
+        r8.forward()
+        r5.far()
+        r9.own()
+        r4.forward()
+    with jax.named_scope("wait_wo"):
+        w_forward(w_f3)
+        pltpu.make_async_copy(osm, wo.at[own_a], l_sem.at[0]).wait()
+        pltpu.make_async_copy(ola, wo.at[own_b], l_sem.at[1]).wait()
+        for yy in (y, yu, yd, y2):
+            for off in (0, 8):
+                s = 2 * yy + 1 - c + off
+                got(wo.at[s], w_rsem.at[s])
+    with jax.named_scope("wait_att"):
+        for s in range(16):
+            got(att.at[s], o_rsem.at[s])
     rows = jnp.concatenate([att[s] for s in range(16)], axis=1)
 
     def project(n, carry):
@@ -398,18 +448,19 @@
     ]
     for d in n_own:
         d.start()
-    r4.forward()
-    r9.forward()
-    for t, k, sends in n_fwd:
-        got(nb.at[t, k], n_rsem.at[t, k])
-        for d in sends:
-            d.start()
-    wt[sp, 0] = gw[...]
-    wt[sp, 1] = uw[...]
-    wt[sp, 2] = dw[...]
-    for ring in (r1, r2, r3, r4, r6, r7, r8, r9):
-        ring.near()
-        ring.far()
+    with jax.named_scope("ev_post2"):
+        r9.forward()
+    with jax.named_scope("wait_nb"):
+        for t, k, sends in n_fwd:
+            got(nb.at[t, k], n_rsem.at[t, k])
+            for d in sends:
+                d.start()
+    for n, a in enumerate((gw, uw, dw)):
+        pltpu.make_async_copy(a, wt.at[sp, n], i_sem.at[6 + n]).wait()
+    with jax.named_scope("wait_w"):
+        for ring in (r1, r2, r3, r4, r6, r7, r8, r9):
+            ring.near()
+            ring.far()
 
     def mixer(groups):
         rows = []
@@ -453,27 +504,33 @@
     r_b = remote(rsend.at[0, 1], tbuf.at[1], r_ssem.at[3], t_rsem.at[1], sp, wd)
     f_a = remote(tbuf.at[0], rrecv.at[2, 0], r_ssem.at[4], r_rsem.at[2], sp, wu)
     f_b = remote(tbuf.at[1], rrecv.at[2, 1], r_ssem.at[5], r_rsem.at[3], sp, wd)
-    mixer([(0, y2)])
-    pair_sum(0)
-    r_a.start()
-    r_b.start()
-    mixer([(1, yu), (2, yd)])
-    got(tbuf.at[0], t_rsem.at[0])
-    f_a.start()
-    got(tbuf.at[1], t_rsem.at[1])
-    f_b.start()
-    pair_sum(1)
-    r_up.start()
-    pair_sum(2)
-    r_down.start()
+    with jax.named_scope("mix0"):
+        mixer([(0, y2)])
+    with jax.named_scope("pair0"):
+        pair_sum(0)
+        r_a.start()
+        r_b.start()
+    with jax.named_scope("mix1"):
+        mixer([(1, yu), (2, yd)])
+    with jax.named_scope("pair12"):
+        got(tbuf.at[0], t_rsem.at[0])
+        f_a.start()
+        got(tbuf.at[1], t_rsem.at[1])
+        f_b.start()
+        pair_sum(1)
+        r_up.start()
+        pair_sum(2)
+        r_down.start()
     mixer_own = [(3, y)]
-    mixer(mixer_own)
+    with jax.named_scope("mix3"):
+        mixer(mixer_own)
     got(precv.at[3], p_rsem.at[3])
     pre[...] = residual_scale * normed.astype(F32) + 0.5 * (mine_f[3] + precv[3].astype(F32))
-    got(rrecv.at[0], r_rsem.at[0])
-    got(rrecv.at[1], r_rsem.at[1])
-    got(rrecv.at[2, 0], r_rsem.at[2])
-    got(rrecv.at[2, 1], r_rsem.at[3])
+    with jax.named_scope("wait_r"):
+        got(rrecv.at[0], r_rsem.at[0])
+        got(rrecv.at[1], r_rsem.at[1])
+        got(rrecv.at[2, 0], r_rsem.at[2])
+        got(rrecv.at[2, 1], r_rsem.at[3])
     for k in range(2):
         cols = pl.ds(1024 * k, 1024)
         more = rrecv[0, k].astype(F32) + rrecv[1, k].astype(F32) + rrecv[2, k].astype(F32)
@@ -518,9 +575,14 @@
         block_kernel,
         name="block",
         out_shape=jax.ShapeDtypeStruct((64, 2048), BF),
-        in_specs=[pl.BlockSpec(memory_space=pltpu.VMEM)] * len(args),
+        in_specs=[
+            pl.BlockSpec(memory_space=pl.ANY if n in (0, 1, 2, 3, 4, 5, 8, 9, 12, 13, 14) else pltpu.VMEM)
+            for n in range(len(args))
+        ],
         out_specs=pl.BlockSpec(memory_space=pltpu.VMEM),
         scratch_shapes=[
+            pltpu.VMEM((CH, 128), BF), pltpu.VMEM((CH, 256), BF), pltpu.VMEM((CH, 128), BF),
+            pltpu.VMEM((CH, 256), BF), pltpu.VMEM((CH, 128), BF), pltpu.VMEM((CH, 128), BF),
             pltpu.VMEM((16, 3, CH, 128), BF),
             pltpu.VMEM((2, 2, CH, 128), BF),
             pltpu.VMEM((2, 2, CH, 128), BF),
@@ -542,9 +604,9 @@
             dma((5,)), dma((2, 3)), dma((5,)), dma((16, 3)), dma((3, 3)), dma((3, 3)), dma((8, 3)),
             dma((3,)), dma((3,)), dma((8,)), dma((16,)), dma((2, 8)), dma((16,)), dma((2,)),
             dma((10, 6)), dma((16, 4)), dma((3,)), dma((3,)), dma((8,)), dma((8, 2)),
-            dma((4,)), dma((4,)), dma((6,)), dma((4,)), dma((2,)),
+            dma((4,)), dma((4,)), dma((6,)), dma((4,)), dma((2,)), dma((9,)),
         ],
-        compiler_params=pltpu.CompilerParams(has_side_effects=True, vmem_limit_bytes=60 * 1024 * 1024),
+        compiler_params=pltpu.CompilerParams(has_side_effects=True, collective_id=0, vmem_limit_bytes=60 * 1024 * 1024),
         cost_estimate=pl.CostEstimate(flops=8 * 10**9, bytes_accessed=10**8, transcendentals=10**7),
     )(*args)
 

time: 130 us -> 121 us (0.931); the launches traced: 130 us -> 119 us
  Pallas kernels: 126 us -> 115 us
    pallas_call x1, Pallas kernels: 126 us -> 115 us  [block(): pl.pallas_call(block_kernel, name='block', out_shape=jax.ShapeDtypeStruct...]
where the time goes in v3:
time: 121 us; the launch traced here: 119 us
  Pallas kernels  115 us (95%)
  local copies, waits for them, and re-layouts  2.34 us (2%)
  between operations  1.31 us (1%)
    pallas_call x1, Pallas kernels, block(): pl.pallas_call(block_kernel, name='block', out_shape=jax.ShapeDtypeStruct...  115 us

profile of v3, /device:TPU:96, one launch (start us, length us, event | category | flops | bytes accessed | tf_op | source)
XLA Modules:
  0.0 119.0 jit_solution(7053078228017298630)
XLA Ops:
  1.3 0.1 maximum_bitcast_fusion
  1.4 0.7 broadcast_in_dim.8.lam_in
  2.0 115.3 %block.1 = bf16[64,2048]{1,0:T(8,128)(2,1)} custom-call(bf16[512,128]{1,0:T(8,128)(2,1)} %bitcast.20, bf16[512,256]{1,0:T(8,128)(2,1)} %bitcast.16, bf16[512,128]{1,0:T(8,128)(2,1)} %bitcast.21, bf16[512,256]{1,0:T(8,128)(2,1)} %bitcast.17, bf16[512,128]{1,0:T(8,128)(2,1)} %bitcast.22, bf16[512,128]{1,0:T(8,128)(2,1)} %bitcast.23, ...), custom_call_target="tpu_custom_call" | custom-call | flops 8000000000 | bytes 100000000 | tf_op jit(solution)/shard_map/block/pallas_call | solution.py:574
  117.3 1.7 %copy.20 = bf16[64,2048]{1,0:T(8,128)(2,1)} copy(bf16[64,2048]{1,0:T(8,128)(2,1)} %block.1) | data formatting | bytes 524288

commit v4 on v3

--- a/solution.py
+++ b/solution.py
@@ -25,12 +25,12 @@
 
 
 def block_kernel(
-    qs_in, ql_in, ks_in, kl_in, vs_in, vl_in, lam_in, gain, osm, ola, res, ngain, gw, uw, dw,
+    qs_in, ql_in, ks_in, kl_in, vs_in, vl_in, lam_s, lam_l, gain, osm, ola, res, ngain, gw, uw, dw,
     out,
-    qs, ql, ks, kl, vs, vl, kv, qb, qz, lam, acc, mx, wo, ob, att, pre, wt, nb, psend, precv, mine_f, rsend, rrecv, tbuf,
+    qs, ql, ks, kl, vs, vl, lam_in, kv, qb, qz, lam, acc, mx, wo, ob, att, pre, wt, nb, psend, precv, mine_f, rsend, rrecv, tbuf, rbuf,
     q_ssem, q_rsem, x_ssem, kv_rsem, up_ssem, dn_ssem, pr_ssem,
     wu_ssem, wd_ssem, wp_ssem, w_rsem, o_ssem, o_rsem, l_sem,
-    g_ssem, g_rsem, nu_ssem, nd_ssem, np_ssem, n_rsem, p_ssem, p_rsem, r_ssem, r_rsem, t_rsem, i_sem,
+    g_ssem, g_rsem, nu_ssem, nd_ssem, np_ssem, n_rsem, p_ssem, p_rsem, r_ssem, r_rsem, t_rsem, i_sem, relay_sem,
 ):
     sp, tp = lax.axis_index("sp"), lax.axis_index("tp")
     z, x, y, c = sp // 4, sp % 4, tp // 2, tp % 2
@@ -71,6 +71,8 @@
     ]
     for d in staged:
         d.start()
+    lam_in[0] = jnp.full((8, 128), lam_s[0], F32)
+    lam_in[1] = jnp.full((8, 128), lam_l[0], F32)
     dcore = 2 * y + x % 2
     small_sp, large_sp = 4 * z + 2 * c, 4 * z + 2 * c + 1
     kv_puts = [
@@ -79,6 +81,15 @@
         (kl.at[:, pl.ds(0, 128)], kv.at[sp, 0], x_ssem.at[2], kv_rsem.at[sp, 0], large_sp, dcore),
         (vl, kv.at[sp, 1], x_ssem.at[3], kv_rsem.at[sp, 1], large_sp, dcore),
         (kl.at[:, pl.ds(128, 128)], kv.at[sp, 2], x_ssem.at[4], kv_rsem.at[sp, 2], large_sp, dcore),
+    ]
+    two_away = (2 * c + 5 - x) % 4 == 2
+    relays = x == 2 * c
+    through = [
+        remote(p[0], rbuf.at[k], p[2], relay_sem.at[k], 4 * z + xu, tp) for k, p in enumerate(kv_puts[2:])
+    ]
+    onward = [
+        remote(rbuf.at[k], kv.at[4 * z + xd, b], relay_sem.at[3 + k], kv_rsem.at[4 * z + xd, b], 4 * z + xu, 2 * y + 1)
+        for k, b in enumerate((0, 1, 2))
     ]
     low = jnp.minimum(sp, 15 - sp)
     hi = sp // 8
@@ -108,18 +119,30 @@
     targets += near + [(a, t) for a in (lo_chunk, hi_chunk) for t in range(8)]
     for d in sources:
         greet(*d)
-    count = len(targets)
+
+    @pl.when(jnp.logical_and(large, c == 1))
+    def _():
+        greet(4 * z + xd, 2 * y + x // 2)
+
+    count = len(targets) + relays.astype(jnp.int32)
     for d in targets:
         count -= jnp.logical_and(d[0] == sp, d[1] == tp).astype(jnp.int32)
     with jax.named_scope("barrier"):
         pl.semaphore_wait(barrier, count)
-    for d, p in zip(staged, (kv_puts[:1], kv_puts[1:2], kv_puts[2:3] + kv_puts[4:], kv_puts[3:4])):
+    for d in staged:
         d.wait()
-        for one in p:
-            put(*one)
-    for d in staged[4:]:
-        d.wait()
-    for p in q_puts:
+
+    @pl.when(two_away)
+    def _():
+        for d in through:
+            d.start()
+
+    @pl.when(jnp.logical_not(two_away))
+    def _():
+        for p in kv_puts[2:]:
+            put(*p)
+
+    for p in q_puts[1:3] + q_puts[4:] + kv_puts[:2] + q_puts[:1] + q_puts[3:4]:
         put(*p)
 
     own_piece = (gw, uw, dw.at[pl.ds(0, 352), :], dw.at[pl.ds(352, 352), :])
@@ -183,7 +206,15 @@
     r1, r2, r3, r4 = [Ring(1 + n, True, 0, line) for n, line in enumerate((z, zd, zu, z2))]
     r5 = Ring(5, True, 2, z)
     r6, r7, r8, r9 = [Ring(6 + n, False, 2, line) for n, line in enumerate((x, xd, xu, x2))]
-    for ring in (r0, r1, r5):
+    r0.own(True)
+
+    @pl.when(relays)
+    def _():
+        for k, d in enumerate(onward):
+            got(rbuf.at[k], relay_sem.at[k])
+            d.start()
+
+    for ring in (r5, r1):
         ring.own(True)
 
     wu, wd = 2 * yu + c, 2 * yd + c
@@ -232,27 +263,40 @@
     factor = jnp.where(large, log2e * 128**-0.5, log2e * 64**-0.5).astype(F32)
     half = CH // 2
 
-    def absorb(h, j, diagonal):
-        values = jnp.concatenate([kv[j, 1], jnp.ones((CH, 128), BF)], axis=1)
-        for m in range(2):
-            keys = kv[j, 2 * m * kind]
-            for t in range(2):
-                rows = pl.ds(t * half, half)
+    def absorb(h, first, shift):
+        subs = [(m, t) for m in range(2) for t in range(2)]
+        values = jnp.concatenate(
+            [jnp.concatenate([kv[first + a, 1], jnp.ones((CH, 128), BF)], axis=1) for a in range(2)], axis=0
+        )
+
+        def scores(m, t):
+            found = []
+            for a in range(2):
                 s = lax.dot_general(
-                    qz[h, m, rows, :], keys, (((1,), (1,)), ((), ())), preferred_element_type=F32
+                    qz[h, m, pl.ds(t * half, half), :], kv[first + a, 2 * m * kind],
+                    (((1,), (1,)), ((), ())), preferred_element_type=F32,
                 )
-                if diagonal:
-                    qi = lax.broadcasted_iota(jnp.int32, (half, CH), 0) + t * half
-                    ki = lax.broadcasted_iota(jnp.int32, (half, CH), 1)
+                if shift is not None:
+                    qi = lax.broadcasted_iota(jnp.int32, (half, CH), 0) + (shift + t * half)
+                    ki = lax.broadcasted_iota(jnp.int32, (half, CH), 1) + a * CH
                     s = jnp.where(ki <= qi, s, masked_score)
-                old = mx[h, m, rows, :]
-                new = jnp.maximum(old, jnp.max(s, axis=1, keepdims=True))
-                mx[h, m, rows, :] = new
-                p = jnp.exp2((s - new[:, :1]) * factor)
-                fade = jnp.exp2((old - new) * factor)
-                pv = jnp.dot(p.astype(BF), values, preferred_element_type=F32)
-                acc[h, m, rows, 0:128] = acc[h, m, rows, 0:128] * fade + pv[:, 0:128]
-                acc[h, m, rows, 128:256] = acc[h, m, rows, 128:256] * fade + pv[:, 128:256]
+                found.append(s)
+            return found, jnp.max(jnp.maximum(found[0], found[1]), axis=1, keepdims=True)
+
+        now = scores(*subs[0])
+        for i, (m, t) in enumerate(subs):
+            later = scores(*subs[i + 1]) if i < 3 else None
+            rows = pl.ds(t * half, half)
+            old = mx[h, m, rows, :]
+            new = jnp.maximum(old, now[1])
+            mx[h, m, rows, :] = new
+            wide = jnp.concatenate([new] * 4, axis=1)
+            p = jnp.concatenate([jnp.exp2((s - wide) * factor).astype(BF) for s in now[0]], axis=1)
+            fade = jnp.exp2((old - new) * factor)
+            pv = jnp.dot(p, values, preferred_element_type=F32)
+            acc[h, m, rows, 0:128] = acc[h, m, rows, 0:128] * fade + pv[:, 0:128]
+            acc[h, m, rows, 128:256] = acc[h, m, rows, 128:256] * fade + pv[:, 128:256]
+            now = later
 
     def kv_send(j, slab, ssem, dsp, dtp):
         return remote(kv.at[j, slab], kv.at[j, slab], ssem, kv_rsem.at[j, slab], dsp, dtp)
@@ -300,12 +344,6 @@
 
     kv_arrive(0)
     kv_arrive(1)
-    with jax.named_scope("ev_pre"):
-        r0.forward()
-        r0.near()
-        r2.own()
-        r3.own()
-        r6.own(True)
     with jax.named_scope("wait_q"):
         for h in range(2):
             got(qb.at[h, 0], q_rsem.at[h, 0])
@@ -324,53 +362,54 @@
                 qz[h, 0] = jnp.where(first, both, jnp.zeros_like(both))
                 qz[h, 1] = jnp.where(first, jnp.zeros_like(both), both)
 
+
     def phase(i, carry):
         level, part, up, down = route(i)
         first = 4 * level + 2 * part
         other = first + 1 - c
 
-        @pl.when(i >= 2)
+        @pl.when((i >= 1) & (i < 7))
         def _():
-            kv_arrive(i)
+            kv_arrive(i + 1)
 
         with jax.named_scope("ev_w"):
+            @pl.when(i == 1)
+            def _():
+                r0.forward()
+                r5.forward()
+                r0.near()
+                r2.own()
+                r3.own()
+
             @pl.when(i == 2)
             def _():
-                r1.forward()
+                w_forward(w_f1)
 
             @pl.when(i == 4)
             def _():
-                r5.forward()
-                r5.near()
-                r7.own()
-                r8.own()
-                r0.far()
-                r4.own()
-                w_forward(w_f1)
+                r6.own(True)
+                w_forward(w_f2)
 
             @pl.when(i == 6)
             def _():
-                r2.forward()
-                r3.forward()
-                w_forward(w_f2)
+                w_forward(w_f3)
 
         with jax.named_scope("wait_kv2"):
             slabs(lambda s: got(kv.at[other, s], kv_rsem.at[other, s]))
-        n_lo = jnp.clip(lo_chunk - first + 1, 0, 2)
-        n_hi = jnp.clip(hi_chunk - first + 1, 0, 2)
+        n_lo = jnp.where(lo_chunk >= first, 1, 0)
+        n_hi = jnp.where(hi_chunk >= first, 1, 0)
 
         def step(k, cc):
             h = jnp.where(k >= n_lo, 1, 0)
-            j = first + k - h * n_lo
-            diagonal = j == jnp.where(h == 1, hi_chunk, lo_chunk)
-
-            @pl.when(diagonal)
-            def _():
-                absorb(h, j, True)
-
-            @pl.when(jnp.logical_not(diagonal))
-            def _():
-                absorb(h, j, False)
+            gap = jnp.where(h == 1, hi_chunk, lo_chunk) - first
+
+            @pl.when(gap < 2)
+            def _():
+                absorb(h, first, gap * CH)
+
+            @pl.when(gap >= 2)
+            def _():
+                absorb(h, first, None)
 
             return cc
 
@@ -395,14 +434,18 @@
             put(ob.at[h, pl.ds(64 * t, 64), :], att.at[slot], o_ssem.at[h, t], o_rsem.at[slot], dsp, t)
 
     with jax.named_scope("ev_post"):
-        r6.forward()
-        r7.forward()
-        r8.forward()
+        r0.far()
+        r4.own()
+        r5.near()
+        r7.own()
+        r8.own()
         r5.far()
         r9.own()
-        r4.forward()
+        r1.forward()
+        r2.forward()
+        r3.forward()
+        r6.forward()
     with jax.named_scope("wait_wo"):
-        w_forward(w_f3)
         pltpu.make_async_copy(osm, wo.at[own_a], l_sem.at[0]).wait()
         pltpu.make_async_copy(ola, wo.at[own_b], l_sem.at[1]).wait()
         for yy in (y, yu, yd, y2):
@@ -448,13 +491,22 @@
     ]
     for d in n_own:
         d.start()
-    with jax.named_scope("ev_post2"):
-        r9.forward()
-    with jax.named_scope("wait_nb"):
-        for t, k, sends in n_fwd:
+    def n_forward(items):
+        for t, k, sends in items:
             got(nb.at[t, k], n_rsem.at[t, k])
             for d in sends:
                 d.start()
+
+    with jax.named_scope("ev_post2"):
+        r7.forward()
+        r8.forward()
+        r4.forward()
+    with jax.named_scope("wait_nb0"):
+        n_forward(n_fwd[:2])
+    with jax.named_scope("ev_post3"):
+        r9.forward()
+    with jax.named_scope("wait_nb"):
+        n_forward(n_fwd[2:])
     for n, a in enumerate((gw, uw, dw)):
         pltpu.make_async_copy(a, wt.at[sp, n], i_sem.at[6 + n]).wait()
     with jax.named_scope("wait_w"):
@@ -492,51 +544,68 @@
     def p_move(g):
         return remote(psend.at[g], precv.at[g], p_ssem.at[g], p_rsem.at[g], sp, partner)
 
-    def pair_sum(g):
-        got(precv.at[g], p_rsem.at[g])
-        both = (mine_f[g] + precv[g].astype(F32)).astype(BF)
-        rsend[g, 0] = both[:, 0:1024]
-        rsend[g, 1] = both[:, 1024:2048]
-
-    r_up = remote(rsend.at[1], rrecv.at[0], r_ssem.at[0], r_rsem.at[0], sp, wu)
-    r_down = remote(rsend.at[2], rrecv.at[1], r_ssem.at[1], r_rsem.at[1], sp, wd)
-    r_a = remote(rsend.at[0, 0], tbuf.at[0], r_ssem.at[2], t_rsem.at[0], sp, wu)
-    r_b = remote(rsend.at[0, 1], tbuf.at[1], r_ssem.at[3], t_rsem.at[1], sp, wd)
-    f_a = remote(tbuf.at[0], rrecv.at[2, 0], r_ssem.at[4], r_rsem.at[2], sp, wu)
-    f_b = remote(tbuf.at[1], rrecv.at[2, 1], r_ssem.at[5], r_rsem.at[3], sp, wd)
+    def pair_sum(g, k):
+        cols = pl.ds(1024 * k, 1024)
+        return mine_f[g, :, cols] + precv[g, :, cols].astype(F32)
+
+    r_a = remote(rsend.at[0, 0], tbuf.at[0], r_ssem.at[0], t_rsem.at[0], sp, wu)
+    r_b = remote(rsend.at[0, 1], tbuf.at[1], r_ssem.at[1], t_rsem.at[1], sp, wd)
+    up_a = remote(rsend.at[1, 0], rrecv.at[0, 0], r_ssem.at[2], r_rsem.at[0], sp, wu)
+    up_b = remote(rsend.at[1, 1], rrecv.at[0, 1], r_ssem.at[3], r_rsem.at[1], sp, wu)
+    down_a = remote(rsend.at[2, 0], rrecv.at[1, 0], r_ssem.at[4], r_rsem.at[2], sp, wd)
+    down_b = remote(rsend.at[2, 1], rrecv.at[1, 1], r_ssem.at[5], r_rsem.at[3], sp, wd)
     with jax.named_scope("mix0"):
         mixer([(0, y2)])
     with jax.named_scope("pair0"):
-        pair_sum(0)
+        got(precv.at[0], p_rsem.at[0])
+        rsend[0, 0] = pair_sum(0, 0).astype(BF)
         r_a.start()
+        rsend[0, 1] = pair_sum(0, 1).astype(BF)
         r_b.start()
     with jax.named_scope("mix1"):
         mixer([(1, yu), (2, yd)])
     with jax.named_scope("pair12"):
+        got(precv.at[1], p_rsem.at[1])
+        rsend[1, 1] = pair_sum(1, 1).astype(BF)
+        up_b.start()
+        got(precv.at[2], p_rsem.at[2])
+        rsend[2, 0] = pair_sum(2, 0).astype(BF)
+        down_a.start()
         got(tbuf.at[0], t_rsem.at[0])
-        f_a.start()
+        rsend[1, 0] = (pair_sum(1, 0) + tbuf[0].astype(F32)).astype(BF)
+        up_a.start()
         got(tbuf.at[1], t_rsem.at[1])
-        f_b.start()
-        pair_sum(1)
-        r_up.start()
-        pair_sum(2)
-        r_down.start()
-    mixer_own = [(3, y)]
+        rsend[2, 1] = (pair_sum(2, 1) + tbuf[1].astype(F32)).astype(BF)
+        down_b.start()
     with jax.named_scope("mix3"):
-        mixer(mixer_own)
+        mixer([(3, y)])
     got(precv.at[3], p_rsem.at[3])
     pre[...] = residual_scale * normed.astype(F32) + 0.5 * (mine_f[3] + precv[3].astype(F32))
     with jax.named_scope("wait_r"):
-        got(rrecv.at[0], r_rsem.at[0])
-        got(rrecv.at[1], r_rsem.at[1])
-        got(rrecv.at[2, 0], r_rsem.at[2])
-        got(rrecv.at[2, 1], r_rsem.at[3])
+        for k in range(2):
+            got(rrecv.at[0, k], r_rsem.at[k])
+            got(rrecv.at[1, k], r_rsem.at[2 + k])
     for k in range(2):
         cols = pl.ds(1024 * k, 1024)
-        more = rrecv[0, k].astype(F32) + rrecv[1, k].astype(F32) + rrecv[2, k].astype(F32)
+        more = rrecv[0, k].astype(F32) + rrecv[1, k].astype(F32)
         out[:, cols] = (pre[:, cols] + 0.5 * more).astype(BF)
 
-    for p in kv_puts:
+    @pl.when(two_away)
+    def _():
+        for d in through:
+            d.wait_send()
+
+    @pl.when(jnp.logical_not(two_away))
+    def _():
+        for p in kv_puts[2:]:
+            put_done(*p)
+
+    @pl.when(relays)
+    def _():
+        for d in onward:
+            d.wait_send()
+
+    for p in kv_puts[:2]:
         put_done(*p)
     for p in q_puts:
         put_done(*p)
@@ -555,7 +624,7 @@
             d.wait_send()
     for g in range(4):
         p_move(g).wait_send()
-    for d in (r_up, r_down, r_a, r_b, f_a, f_b):
+    for d in (r_a, r_b, up_a, up_b, down_a, down_b):
         d.wait_send()
 
     def drain(i, carry):
@@ -576,13 +645,14 @@
         name="block",
         out_shape=jax.ShapeDtypeStruct((64, 2048), BF),
         in_specs=[
-            pl.BlockSpec(memory_space=pl.ANY if n in (0, 1, 2, 3, 4, 5, 8, 9, 12, 13, 14) else pltpu.VMEM)
-            for n in range(len(args))
+            pl.BlockSpec(memory_space={"h": pl.ANY, "v": pltpu.VMEM, "s": pltpu.SMEM}[k])
+            for k in "hhhhhhssvhhvvhhh"
         ],
         out_specs=pl.BlockSpec(memory_space=pltpu.VMEM),
         scratch_shapes=[
             pltpu.VMEM((CH, 128), BF), pltpu.VMEM((CH, 256), BF), pltpu.VMEM((CH, 128), BF),
             pltpu.VMEM((CH, 256), BF), pltpu.VMEM((CH, 128), BF), pltpu.VMEM((CH, 128), BF),
+            pltpu.VMEM((2, 8, 128), F32),
             pltpu.VMEM((16, 3, CH, 128), BF),
             pltpu.VMEM((2, 2, CH, 128), BF),
             pltpu.VMEM((2, 2, CH, 128), BF),
@@ -599,12 +669,13 @@
             pltpu.VMEM((4, 64, 2048), BF),
             pltpu.VMEM((4, 64, 2048), F32),
             pltpu.VMEM((3, 2, 64, 1024), BF),
-            pltpu.VMEM((3, 2, 64, 1024), BF),
+            pltpu.VMEM((2, 2, 64, 1024), BF),
             pltpu.VMEM((2, 64, 1024), BF),
+            pltpu.VMEM((3, CH, 128), BF),
             dma((5,)), dma((2, 3)), dma((5,)), dma((16, 3)), dma((3, 3)), dma((3, 3)), dma((8, 3)),
             dma((3,)), dma((3,)), dma((8,)), dma((16,)), dma((2, 8)), dma((16,)), dma((2,)),
             dma((10, 6)), dma((16, 4)), dma((3,)), dma((3,)), dma((8,)), dma((8, 2)),
-            dma((4,)), dma((4,)), dma((6,)), dma((4,)), dma((2,)), dma((9,)),
+            dma((4,)), dma((4,)), dma((6,)), dma((4,)), dma((2,)), dma((9,)), dma((6,)),
         ],
         compiler_params=pltpu.CompilerParams(has_side_effects=True, collective_id=0, vmem_limit_bytes=60 * 1024 * 1024),
         cost_estimate=pl.CostEstimate(flops=8 * 10**9, bytes_accessed=10**8, transcendentals=10**7),
@@ -617,10 +688,9 @@
     gate_weight, up_weight, down_weight,
 ):
     flat = lambda a: a.reshape(a.shape[0], a.shape[2])
-    lam = jnp.broadcast_to(jnp.stack([lambda_small, lambda_large]).reshape(2, 1, 1), (2, 8, 128))
     return block(
         flat(query_small), flat(query_large), flat(key_small), flat(key_large), flat(value_small),
-        flat(value_large), lam, head_gain.reshape(1, 128), output_small, output_large, residual,
+        flat(value_large), lambda_small, lambda_large, head_gain.reshape(1, 128), output_small, output_large, residual,
         norm_gain.reshape(1, 2048), gate_weight.T, up_weight.T, down_weight,
     )
 

time: 121 us -> 109 us (0.901)
  Pallas kernels: 115 us -> 105 us
    pallas_call x1, Pallas kernels: 115 us -> 105 us  [block(): pl.pallas_call(block_kernel, name='block', out_shape=jax.ShapeDtypeStruct...]
where the time goes in v4:
time: 109 us; the launch traced here: 108 us
  Pallas kernels  105 us (96%)
  local copies, waits for them, and re-layouts  1.67 us (2%)
  between operations  1.31 us (1%)
    pallas_call x1, Pallas kernels, block(): pl.pallas_call(block_kernel, name='block', out_shape=jax.ShapeDtypeStruct...  105 us

profile of v4, /device:TPU:96, one launch (start us, length us, event | category | flops | bytes accessed | tf_op | source)
XLA Modules:
  0.0 107.8 jit_solution(750289858816546034)
XLA Ops:
  1.3 104.9 %block.1 = bf16[64,2048]{1,0:T(8,128)(2,1)} custom-call(bf16[512,128]{1,0:T(8,128)(2,1)} %bitcast.14, bf16[512,256]{1,0:T(8,128)(2,1)} %bitcast.10, bf16[512,128]{1,0:T(8,128)(2,1)} %bitcast.15, bf16[512,256]{1,0:T(8,128)(2,1)} %bitcast.11, bf16[512,128]{1,0:T(8,128)(2,1)} %bitcast.16, bf16[512,128]{1,0:T(8,128)(2,1)} %bitcast.17, f32[1]{0:T(128)S(6)} %copy.18.lam_s, ...), custom_call_target="tpu_custom_call" | custom-call | flops 8000000000 | bytes 100000000 | tf_op jit(solution)/shard_map/block/pallas_call | solution.py:643
  106.2 1.7 %copy.20 = bf16[64,2048]{1,0:T(8,128)(2,1)} copy(bf16[64,2048]{1,0:T(8,128)(2,1)} %block.1) | data formatting | bytes 524288

commit v5 on v4

--- a/solution.py
+++ b/solution.py
@@ -25,9 +25,9 @@
 
 
 def block_kernel(
-    qs_in, ql_in, ks_in, kl_in, vs_in, vl_in, lam_s, lam_l, gain, osm, ola, res, ngain, gw, uw, dw,
+    qs_in, ql_in, ks_in, kl_in, vs_in, vl_in, lam_s, lam_l, gain_in, osm, ola, res_in, ngain_in, gw, uw, dw,
     out,
-    qs, ql, ks, kl, vs, vl, lam_in, kv, qb, qz, lam, acc, mx, wo, ob, att, pre, wt, nb, psend, precv, mine_f, rsend, rrecv, tbuf, rbuf,
+    qs, ql, ks, kl, vs, vl, lam_in, gain, res, ngain, kv, qb, qz, lam, acc, mx, wo, ob, att, pre, wt, nb, psend, precv, mine_f, rsend, rrecv, tbuf, rbuf,
     q_ssem, q_rsem, x_ssem, kv_rsem, up_ssem, dn_ssem, pr_ssem,
     wu_ssem, wd_ssem, wp_ssem, w_rsem, o_ssem, o_rsem, l_sem,
     g_ssem, g_rsem, nu_ssem, nd_ssem, np_ssem, n_rsem, p_ssem, p_rsem, r_ssem, r_rsem, t_rsem, i_sem, relay_sem,
@@ -39,7 +39,7 @@
     zu, zd, z2 = (z + 1) % 4, (z + 3) % 4, (z + 2) % 4
     yu, yd, y2 = (y + 1) % 4, (y + 3) % 4, (y + 2) % 4
     xu, xd, x2 = (x + 1) % 4, (x + 3) % 4, (x + 2) % 4
-    r = 2 * (3 - z) + c
+    r = 2 * jnp.where(z < 2, 3 - z, z - 2) + c
     lo_chunk, hi_chunk = r, 15 - r
 
     def put(src, dst, ssem, rsem, dsp, dtp):
@@ -70,6 +70,12 @@
         )
     ]
     for d in staged:
+        d.start()
+    small_in = [
+        pltpu.make_async_copy(a, b, i_sem.at[9 + n])
+        for n, (a, b) in enumerate(((gain_in, gain), (res_in, res), (ngain_in, ngain)))
+    ]
+    for d in small_in:
         d.start()
     lam_in[0] = jnp.full((8, 128), lam_s[0], F32)
     lam_in[1] = jnp.full((8, 128), lam_l[0], F32)
@@ -93,7 +99,8 @@
     ]
     low = jnp.minimum(sp, 15 - sp)
     hi = sp // 8
-    qsp = 4 * (3 - low // 2) + 2 * c
+    qz_at = jnp.where(low < 4, low // 2 + 2, 3 - low // 2)
+    qsp = 4 * qz_at + 2 * c
     qtp = 2 * y + low % 2
     q_puts = [
         (qs, qb.at[hi, 0], q_ssem.at[0], q_rsem.at[hi, 0], qsp, qtp),
@@ -115,7 +122,7 @@
     targets += [(qsp, qtp), (qsp + 1, qtp)]
     near = [(4 * zu + x, tp), (4 * zd + x, tp), (4 * z + xu, tp), (4 * z + xd, tp)]
     near += [(sp, 2 * yu + c), (sp, 2 * yd + c), (sp, 2 * y + 1 - c)]
-    sources += near + [(4 * (3 - low // 2) + a, 2 * b + low % 2) for a in range(4) for b in range(4)]
+    sources += near + [(4 * qz_at + a, 2 * b + low % 2) for a in range(4) for b in range(4)]
     targets += near + [(a, t) for a in (lo_chunk, hi_chunk) for t in range(8)]
     for d in sources:
         greet(*d)
@@ -190,6 +197,10 @@
             self.got(2, self.first + 1)
             f2.start()
 
+        def first_far(self):
+            self.got(1, self.first)
+            self.got(2, self.first + 1)
+
         def near(self):
             self.got(1, self.first + 1)
             self.got(2, self.first)
@@ -214,8 +225,6 @@
             got(rbuf.at[k], relay_sem.at[k])
             d.start()
 
-    for ring in (r5, r1):
-        ring.own(True)
 
     wu, wd = 2 * yu + c, 2 * yd + c
     partner = 2 * y + 1 - c
@@ -298,129 +307,9 @@
             acc[h, m, rows, 128:256] = acc[h, m, rows, 128:256] * fade + pv[:, 128:256]
             now = later
 
-    def kv_send(j, slab, ssem, dsp, dtp):
-        return remote(kv.at[j, slab], kv.at[j, slab], ssem, kv_rsem.at[j, slab], dsp, dtp)
-
-    def slabs(fn):
-        fn(0)
-        fn(1)
-
-        @pl.when(large)
-        def _():
-            fn(2)
-
-    def route(i):
-        own = i < 2
-        off = jnp.where(own, 0, jnp.where((i == 2) | (i == 4), 3, jnp.where(i < 6, 1, 2)))
-        part = jnp.where((i == 0) | (i == 2) | (i == 5) | (i == 6), 0, 1)
-        level = (z + off) % 4
-        up = own | (i == 2)
-        down = own | (i == 3)
-        return level, part, up, down
-
-    def kv_moves(i, act):
-        level, part, up, down = route(i)
-        j = 4 * level + 2 * part + c
-
-        def one(s):
-            @pl.when(up)
-            def _():
-                act(kv_send(j, s, up_ssem.at[jnp.minimum(i, 2), s], 4 * zu + x, tp))
-
-            @pl.when(down)
-            def _():
-                act(kv_send(j, s, dn_ssem.at[jnp.minimum(i, 2), s], 4 * zd + x, tp))
-
-            act(kv_send(j, s, pr_ssem.at[i, s], sp, partner))
-
-        slabs(one)
-
-    def kv_arrive(i):
-        level, part, up, down = route(i)
-        mine = 4 * level + 2 * part + c
-        with jax.named_scope("wait_kv"):
-            slabs(lambda s: got(kv.at[mine, s], kv_rsem.at[mine, s]))
-        kv_moves(i, lambda d: d.start())
-
-    kv_arrive(0)
-    kv_arrive(1)
-    with jax.named_scope("wait_q"):
-        for h in range(2):
-            got(qb.at[h, 0], q_rsem.at[h, 0])
-            got(lam.at[h], q_rsem.at[h, 2])
-
-            @pl.when(large)
-            def _():
-                got(qb.at[h, 1], q_rsem.at[h, 1])
-                qz[h, 0] = qb[h, 0]
-                qz[h, 1] = qb[h, 1]
-
-            @pl.when(jnp.logical_not(large))
-            def _():
-                both = qb[h, 0]
-                first = lax.broadcasted_iota(jnp.int32, (CH, 128), 1) < 64
-                qz[h, 0] = jnp.where(first, both, jnp.zeros_like(both))
-                qz[h, 1] = jnp.where(first, jnp.zeros_like(both), both)
-
-
-    def phase(i, carry):
-        level, part, up, down = route(i)
-        first = 4 * level + 2 * part
-        other = first + 1 - c
-
-        @pl.when((i >= 1) & (i < 7))
-        def _():
-            kv_arrive(i + 1)
-
-        with jax.named_scope("ev_w"):
-            @pl.when(i == 1)
-            def _():
-                r0.forward()
-                r5.forward()
-                r0.near()
-                r2.own()
-                r3.own()
-
-            @pl.when(i == 2)
-            def _():
-                w_forward(w_f1)
-
-            @pl.when(i == 4)
-            def _():
-                r6.own(True)
-                w_forward(w_f2)
-
-            @pl.when(i == 6)
-            def _():
-                w_forward(w_f3)
-
-        with jax.named_scope("wait_kv2"):
-            slabs(lambda s: got(kv.at[other, s], kv_rsem.at[other, s]))
-        n_lo = jnp.where(lo_chunk >= first, 1, 0)
-        n_hi = jnp.where(hi_chunk >= first, 1, 0)
-
-        def step(k, cc):
-            h = jnp.where(k >= n_lo, 1, 0)
-            gap = jnp.where(h == 1, hi_chunk, lo_chunk) - first
-
-            @pl.when(gap < 2)
-            def _():
-                absorb(h, first, gap * CH)
-
-            @pl.when(gap >= 2)
-            def _():
-                absorb(h, first, None)
-
-            return cc
-
-        with jax.named_scope("attn"):
-            lax.fori_loop(0, n_lo + n_hi, step, 0)
-        return carry
-
-    lax.fori_loop(0, 8, phase, 0)
-
     slot = 8 * kind + 2 * y + x // 2
-    for h in range(2):
+
+    def finish(h):
         for t in range(2):
             rows = pl.ds(t * half, half)
             one = acc[h, 0, rows, 0:128] / acc[h, 0, rows, 128:256]
@@ -433,6 +322,149 @@
         for t in range(8):
             put(ob.at[h, pl.ds(64 * t, 64), :], att.at[slot], o_ssem.at[h, t], o_rsem.at[slot], dsp, t)
 
+    def kv_send(j, slab, ssem, dsp, dtp):
+        return remote(kv.at[j, slab], kv.at[j, slab], ssem, kv_rsem.at[j, slab], dsp, dtp)
+
+    def slabs(fn):
+        fn(0)
+        fn(1)
+
+        @pl.when(large)
+        def _():
+            fn(2)
+
+    def route(i):
+        own = i < 2
+        off = jnp.where(own, 0, jnp.where((i == 2) | (i == 4), 3, jnp.where(i < 6, 1, 2)))
+        part = jnp.where((i == 0) | (i == 2) | (i == 5) | (i == 6), 0, 1)
+        level = (z + off) % 4
+        up = own | (i == 2)
+        down = own | (i == 3)
+        return level, part, up, down
+
+    def kv_moves(i, act):
+        level, part, up, down = route(i)
+        j = 4 * level + 2 * part + c
+
+        def one(s):
+            @pl.when(up)
+            def _():
+                act(kv_send(j, s, up_ssem.at[jnp.minimum(i, 2), s], 4 * zu + x, tp))
+
+            @pl.when(down)
+            def _():
+                act(kv_send(j, s, dn_ssem.at[jnp.minimum(i, 2), s], 4 * zd + x, tp))
+
+            act(kv_send(j, s, pr_ssem.at[i, s], sp, partner))
+
+        slabs(one)
+
+    def kv_arrive(i):
+        level, part, up, down = route(i)
+        mine = 4 * level + 2 * part + c
+        with jax.named_scope("wait_kv"):
+            slabs(lambda s: got(kv.at[mine, s], kv_rsem.at[mine, s]))
+        kv_moves(i, lambda d: d.start())
+
+    kv_arrive(0)
+    kv_arrive(1)
+    r5.own(True)
+    r1.own(True)
+    for d in small_in:
+        d.wait()
+    with jax.named_scope("wait_q"):
+        for h in range(2):
+            got(qb.at[h, 0], q_rsem.at[h, 0])
+            got(lam.at[h], q_rsem.at[h, 2])
+
+            @pl.when(large)
+            def _():
+                got(qb.at[h, 1], q_rsem.at[h, 1])
+                qz[h, 0] = qb[h, 0]
+                qz[h, 1] = qb[h, 1]
+
+            @pl.when(jnp.logical_not(large))
+            def _():
+                both = qb[h, 0]
+                first = lax.broadcasted_iota(jnp.int32, (CH, 128), 1) < 64
+                qz[h, 0] = jnp.where(first, both, jnp.zeros_like(both))
+                qz[h, 1] = jnp.where(first, jnp.zeros_like(both), both)
+
+
+    def phase(i, carry):
+        level, part, up, down = route(i)
+        first = 4 * level + 2 * part
+        other = first + 1 - c
+
+        @pl.when((i >= 1) & (i < 5))
+        def _():
+            kv_arrive(i + 1)
+
+        with jax.named_scope("ev_w"):
+            @pl.when(i == 1)
+            def _():
+                r0.first_far()
+                r5.forward()
+                r0.near()
+                r2.own()
+                r3.own()
+
+            @pl.when(i == 2)
+            def _():
+                for d in r0.far_sends():
+                    d.start()
+                w_forward(w_f1)
+
+            @pl.when(i == 4)
+            def _():
+                r6.own(True)
+                r1.forward()
+                w_forward(w_f2)
+
+            @pl.when(i == 6)
+            def _():
+                @pl.when(z != 2)
+                def _():
+                    finish(0)
+
+                w_forward(w_f3)
+
+        with jax.named_scope("wait_kv2"):
+            slabs(lambda s: got(kv.at[other, s], kv_rsem.at[other, s]))
+        n_lo = jnp.where(lo_chunk >= first, 1, 0)
+        n_hi = jnp.where(hi_chunk >= first, 1, 0)
+
+        def step(k, cc):
+            h = jnp.where(k >= n_lo, 1, 0)
+            gap = jnp.where(h == 1, hi_chunk, lo_chunk) - first
+
+            @pl.when(gap < 2)
+            def _():
+                absorb(h, first, gap * CH)
+
+            @pl.when(gap >= 2)
+            def _():
+                absorb(h, first, None)
+
+            return cc
+
+        with jax.named_scope("attn"):
+            lax.fori_loop(0, n_lo + n_hi, step, 0)
+
+        @pl.when(i == 5)
+        def _():
+            kv_arrive(6)
+            kv_arrive(7)
+
+        return carry
+
+    lax.fori_loop(0, 8, phase, 0)
+
+    @pl.when(z == 2)
+    def _():
+        finish(0)
+
+    finish(1)
     with jax.named_scope("ev_post"):
         r0.far()
         r4.own()
@@ -441,7 +473,6 @@
         r8.own()
         r5.far()
         r9.own()
-        r1.forward()
         r2.forward()
         r3.forward()
         r6.forward()
@@ -452,20 +483,17 @@
             for off in (0, 8):
                 s = 2 * yy + 1 - c + off
                 got(wo.at[s], w_rsem.at[s])
-    with jax.named_scope("wait_att"):
-        for s in range(16):
-            got(att.at[s], o_rsem.at[s])
-    rows = jnp.concatenate([att[s] for s in range(16)], axis=1)
-
-    def project(n, carry):
-        cols = pl.ds(pl.multiple_of(n * 512, 512), 512)
-        w = wo[:, :, cols].reshape(2048, 512)
-        pre[:, cols] = residual_scale * res[:, cols].astype(F32) + jnp.dot(
-            rows, w, preferred_element_type=F32
-        )
-        return carry
-
-    lax.fori_loop(0, 4, project, 0)
+    pre[...] = residual_scale * res[...].astype(F32)
+    for part in range(2):
+        with jax.named_scope("wait_att"):
+            for s in range(8 * part, 8 * part + 8):
+                got(att.at[s], o_rsem.at[s])
+        rows = jnp.concatenate([att[s] for s in range(8 * part, 8 * part + 8)], axis=1)
+        for n in range(4):
+            cols = pl.ds(512 * n, 512)
+            w = wo[8 * part : 8 * part + 8, :, cols].reshape(1024, 512)
+            pre[:, cols] += jnp.dot(rows, w, preferred_element_type=F32)
+
     values = pre[...]
     centered = values - jnp.mean(values, axis=1, keepdims=True)
     variance = jnp.mean(centered * centered, axis=1, keepdims=True)
@@ -643,16 +671,17 @@
     return pl.pallas_call(
         block_kernel,
         name="block",
-        out_shape=jax.ShapeDtypeStruct((64, 2048), BF),
+        out_shape=pltpu.VMEM((64, 2048), BF),
         in_specs=[
             pl.BlockSpec(memory_space={"h": pl.ANY, "v": pltpu.VMEM, "s": pltpu.SMEM}[k])
-            for k in "hhhhhhssvhhvvhhh"
+            for k in "hhhhhhsshhhhhhhh"
         ],
         out_specs=pl.BlockSpec(memory_space=pltpu.VMEM),
         scratch_shapes=[
             pltpu.VMEM((CH, 128), BF), pltpu.VMEM((CH, 256), BF), pltpu.VMEM((CH, 128), BF),
             pltpu.VMEM((CH, 256), BF), pltpu.VMEM((CH, 128), BF), pltpu.VMEM((CH, 128), BF),
-            pltpu.VMEM((2, 8, 128), F32),
+            pltpu.VMEM((2, 8, 128), F32), pltpu.VMEM((1, 128), F32), pltpu.VMEM((64, 2048), BF),
+            pltpu.VMEM((1, 2048), F32),
             pltpu.VMEM((16, 3, CH, 128), BF),
             pltpu.VMEM((2, 2, CH, 128), BF),
             pltpu.VMEM((2, 2, CH, 128), BF),
@@ -675,7 +704,7 @@
             dma((5,)), dma((2, 3)), dma((5,)), dma((16, 3)), dma((3, 3)), dma((3, 3)), dma((8, 3)),
             dma((3,)), dma((3,)), dma((8,)), dma((16,)), dma((2, 8)), dma((16,)), dma((2,)),
             dma((10, 6)), dma((16, 4)), dma((3,)), dma((3,)), dma((8,)), dma((8, 2)),
-            dma((4,)), dma((4,)), dma((6,)), dma((4,)), dma((2,)), dma((9,)), dma((6,)),
+            dma((4,)), dma((4,)), dma((6,)), dma((4,)), dma((2,)), dma((12,)), dma((6,)),
         ],
         compiler_params=pltpu.CompilerParams(has_side_effects=True, collective_id=0, vmem_limit_bytes=60 * 1024 * 1024),
         cost_estimate=pl.CostEstimate(flops=8 * 10**9, bytes_accessed=10**8, transcendentals=10**7),

time: 109 us -> 105 us (0.963); the launches traced: 108 us -> 103 us
  Pallas kernels: 105 us -> 101 us
    pallas_call x1, Pallas kernels: 105 us -> 101 us  [block(): pl.pallas_call(block_kernel, name='block', out_shape=pltpu.VMEM((64, 2048...]
where the time goes in v5:
time: 105 us; the launch traced here: 103 us
  Pallas kernels  101 us (96%)
  between operations  1.31 us (1%)
    pallas_call x1, Pallas kernels, block(): pl.pallas_call(block_kernel, name='block', out_shape=pltpu.VMEM((64, 2048...  101 us

profile of v5, /device:TPU:96, one launch (start us, length us, event | category | flops | bytes accessed | tf_op | source)
XLA Modules:
  0.0 102.6 jit_solution(12143542442230880390)
XLA Ops:
  1.3 100.5 %block.1 = bf16[64,2048]{1,0:T(8,128)(2,1)S(1)} custom-call(bf16[512,128]{1,0:T(8,128)(2,1)} %bitcast.14, bf16[512,256]{1,0:T(8,128)(2,1)} %bitcast.10, bf16[512,128]{1,0:T(8,128)(2,1)} %bitcast.15, bf16[512,256]{1,0:T(8,128)(2,1)} %bitcast.11, bf16[512,128]{1,0:T(8,128)(2,1)} %bitcast.16, bf16[512,128]{1,0:T(8,128)(2,1)} %bitcast.17, f32[1]{0:T(128)S(6)} %copy.19.lam_s, ...), custom_call_target="tpu_custom_call" | custom-call | flops 8000000000 | bytes 100000000 | tf_op jit(solution)/shard_map/block/pallas_call | solution.py:671
  101.9 0.7 copy.18

commit v6 on v5

--- a/solution.py
+++ b/solution.py
@@ -318,9 +318,9 @@
             square = jnp.mean(combined * combined, axis=1, keepdims=True)
             normed = combined * lax.rsqrt(square + norm_epsilon) * gain[...] * branch_scale
             ob[h, rows, :] = normed.astype(BF)
-        dsp = hi_chunk if h == 1 else lo_chunk
-        for t in range(8):
-            put(ob.at[h, pl.ds(64 * t, 64), :], att.at[slot], o_ssem.at[h, t], o_rsem.at[slot], dsp, t)
+            dsp = hi_chunk if h == 1 else lo_chunk
+            for n in range(4 * t, 4 * t + 4):
+                put(ob.at[h, pl.ds(64 * n, 64), :], att.at[slot], o_ssem.at[h, n], o_rsem.at[slot], dsp, n)
 
     def kv_send(j, slab, ssem, dsp, dtp):
         return remote(kv.at[j, slab], kv.at[j, slab], ssem, kv_rsem.at[j, slab], dsp, dtp)
@@ -542,7 +542,7 @@
             ring.near()
             ring.far()
 
-    def mixer(groups):
+    def mixer(groups, between=None):
         rows = []
         for g, yy in groups:
             t = 2 * yy + 1 - c
@@ -555,6 +555,8 @@
         gate = lax.dot_general(
             rows, jnp.concatenate([wt[s, 0] for s in range(16)], axis=1), nt, preferred_element_type=F32
         )
+        if between is not None:
+            between()
         up = lax.dot_general(
             rows, jnp.concatenate([wt[s, 1] for s in range(16)], axis=1), nt, preferred_element_type=F32
         )
@@ -584,40 +586,33 @@
     down_b = remote(rsend.at[2, 1], rrecv.at[1, 1], r_ssem.at[5], r_rsem.at[3], sp, wd)
     with jax.named_scope("mix0"):
         mixer([(0, y2)])
-    with jax.named_scope("pair0"):
-        got(precv.at[0], p_rsem.at[0])
-        rsend[0, 0] = pair_sum(0, 0).astype(BF)
-        r_a.start()
-        rsend[0, 1] = pair_sum(0, 1).astype(BF)
-        r_b.start()
-    with jax.named_scope("mix1"):
-        mixer([(1, yu), (2, yd)])
-    with jax.named_scope("pair12"):
-        got(precv.at[1], p_rsem.at[1])
-        rsend[1, 1] = pair_sum(1, 1).astype(BF)
-        up_b.start()
-        got(precv.at[2], p_rsem.at[2])
-        rsend[2, 0] = pair_sum(2, 0).astype(BF)
-        down_a.start()
-        got(tbuf.at[0], t_rsem.at[0])
-        rsend[1, 0] = (pair_sum(1, 0) + tbuf[0].astype(F32)).astype(BF)
-        up_a.start()
-        got(tbuf.at[1], t_rsem.at[1])
-        rsend[2, 1] = (pair_sum(2, 1) + tbuf[1].astype(F32)).astype(BF)
-        down_b.start()
-    with jax.named_scope("mix3"):
-        mixer([(3, y)])
+    def pass_far():
+        with jax.named_scope("pair0"):
+            got(precv.at[0], p_rsem.at[0])
+            rsend[0, 0] = pair_sum(0, 0).astype(BF)
+            r_a.start()
+            rsend[0, 1] = pair_sum(0, 1).astype(BF)
+            r_b.start()
+
+    def pass_near():
+        with jax.named_scope("pair12"):
+            got(precv.at[1], p_rsem.at[1])
+            rsend[1, 1] = pair_sum(1, 1).astype(BF)
+            up_b.start()
+            got(precv.at[2], p_rsem.at[2])
+            rsend[2, 0] = pair_sum(2, 0).astype(BF)
+            down_a.start()
+            got(tbuf.at[0], t_rsem.at[0])
+            rsend[1, 0] = (pair_sum(1, 0) + tbuf[0].astype(F32)).astype(BF)
+            up_a.start()
+            got(tbuf.at[1], t_rsem.at[1])
+            rsend[2, 1] = (pair_sum(2, 1) + tbuf[1].astype(F32)).astype(BF)
+            down_b.start()
+
+    mixer([(1, yu), (2, yd)], pass_far)
+    mixer([(3, y)], pass_near)
     got(precv.at[3], p_rsem.at[3])
     pre[...] = residual_scale * normed.astype(F32) + 0.5 * (mine_f[3] + precv[3].astype(F32))
-    with jax.named_scope("wait_r"):
-        for k in range(2):
-            got(rrecv.at[0, k], r_rsem.at[k])
-            got(rrecv.at[1, k], r_rsem.at[2 + k])
-    for k in range(2):
-        cols = pl.ds(1024 * k, 1024)
-        more = rrecv[0, k].astype(F32) + rrecv[1, k].astype(F32)
-        out[:, cols] = (pre[:, cols] + 0.5 * more).astype(BF)
-
     @pl.when(two_away)
     def _():
         for d in through:
@@ -652,8 +647,6 @@
             d.wait_send()
     for g in range(4):
         p_move(g).wait_send()
-    for d in (r_a, r_b, up_a, up_b, down_a, down_b):
-        d.wait_send()
 
     def drain(i, carry):
         kv_moves(i, lambda d: d.wait_send())
@@ -664,6 +657,18 @@
         dsp = hi_chunk if h == 1 else lo_chunk
         for t in range(8):
             put_done(ob.at[h, pl.ds(64 * t, 64), :], att.at[slot], o_ssem.at[h, t], o_rsem.at[slot], dsp, t)
+
+    with jax.named_scope("wait_r"):
+        got(rrecv.at[0, 1], r_rsem.at[1])
+        got(rrecv.at[1, 0], r_rsem.at[2])
+        pre[:, 1024:2048] += 0.5 * rrecv[0, 1].astype(F32)
+        pre[:, 0:1024] += 0.5 * rrecv[1, 0].astype(F32)
+        got(rrecv.at[0, 0], r_rsem.at[0])
+        out[:, 0:1024] = (pre[:, 0:1024] + 0.5 * rrecv[0, 0].astype(F32)).astype(BF)
+        got(rrecv.at[1, 1], r_rsem.at[3])
+        out[:, 1024:2048] = (pre[:, 1024:2048] + 0.5 * rrecv[1, 1].astype(F32)).astype(BF)
+    for d in (r_a, r_b, up_a, up_b, down_a, down_b):
+        d.wait_send()
 
 
 def block(*args):

time: 105 us -> 104 us (level)
  the two profiles are of different devices: /device:TPU:96 before, /device:TPU:1 now
where the time goes in v6:
time: 104 us
  Pallas kernels  102 us (98%)
  between operations  1.31 us (1%)
    pallas_call x1, Pallas kernels, block(): pl.pallas_call(block_kernel, name='block', out_shape=pltpu.VMEM((64, 2048...  102 us

profile of v6, /device:TPU:1, one launch (start us, length us, event | category | flops | bytes accessed | tf_op | source)
XLA Modules:
  0.0 104.0 jit_solution(10423169664708963530)
XLA Ops:
  1.3 102.0 %block.1 = bf16[64,2048]{1,0:T(8,128)(2,1)S(1)} custom-call(bf16[512,128]{1,0:T(8,128)(2,1)} %bitcast.14, bf16[512,256]{1,0:T(8,128)(2,1)} %bitcast.10, bf16[512,128]{1,0:T(8,128)(2,1)} %bitcast.15, bf16[512,256]{1,0:T(8,128)(2,1)} %bitcast.11, bf16[512,128]{1,0:T(8,128)(2,1)} %bitcast.16, bf16[512,128]{1,0:T(8,128)(2,1)} %bitcast.17, f32[1]{0:T(128)S(6)} %copy.19.lam_s, ...), custom_call_target="tpu_custom_call" | custom-call | flops 8000000000 | bytes 100000000 | tf_op jit(solution)/shard_map/block/pallas_call | solution.py:676
  103.3 0.7 copy.18
